TPU v7x, 1024 devices: a whole 4x4x32 slice. The times are simulated.
1024 devices in a mesh: ep: 64 (over z, core), tp: 16 (over y, x).
Axes of the slice: x: 4, y: 4, z: 32, core: 2. Of those that a mesh axis runs over, the one named last changes fastest.
Arguments:
- tokens: bfloat16 [8192, 2048], P('ep'), may hold values from -6 to 6
- chosen: int32 [64, 64, 8], replicated, may hold values from 0 to 127, as said below
- chosen_weight: float32 [64, 64, 8], P('ep'), may hold values from 0.1 to 1
- gate_weight: bfloat16 [64, 2048, 4096], P('ep', None, 'tp'), may hold values from -0.125 to 0.125
- up_weight: bfloat16 [64, 2048, 4096], P('ep', None, 'tp'), may hold values from -0.125 to 0.125
- down_weight: bfloat16 [64, 4096, 2048], P('ep', 'tp'), may hold values from -0.09375 to 0.09375
Outputs:
- combined: bfloat16 [8192, 2048], P('ep', 'tp')
Inputs may be any that keep to these rules, and one draw needn't show every extreme that they name: `chosen`: for every block and expert the 8 positions are distinct.
All inputs are finite; a program needn't handle non-finite values.
Results may differ from a plain program's by a relative error of at most 0.015.
Values may be sent and summed in bfloat16 or wider, within the bound.
No kernel may reach another device: no remote copies, remote signals or barrier semaphores. Data moves between devices by JAX's collectives and lax.ppermute only.
A program may use at most 32 MiB of HBM per device.

v0:
```python
import jax
import jax.numpy as jnp
from jax import lax
from jax.sharding import PartitionSpec as P


def from_everyone(shard, axis):
    copies = jnp.broadcast_to(shard, (lax.axis_size(axis), *shard.shape))
    return lax.all_to_all(copies, axis, split_axis=0, concat_axis=0, tiled=True)


def in_order(tiles, dim):
    tiles = jnp.moveaxis(tiles, 0, dim)
    lengths = tiles.shape
    return tiles.reshape(*lengths[:dim], lengths[dim] * lengths[dim + 1], *lengths[dim + 2 :])


def gathered_copies(shard, axis, dim):
    tiles = from_everyone(shard, axis)
    return in_order(tiles, dim)


def split_up(shard, dim, size):
    lengths = shard.shape
    tiles = shard.reshape(*lengths[:dim], size, lengths[dim] // size, *lengths[dim + 1 :])
    return jnp.moveaxis(tiles, dim, 0)


def sent_and_summed(shard, axis, dim):
    tiles = split_up(shard, dim, lax.axis_size(axis))
    arrived = lax.all_to_all(tiles, axis, split_axis=0, concat_axis=0, tiled=True)
    return arrived.astype(jnp.float32).sum(axis=0)


def local(tokens, chosen, chosen_weight, gate_weight, up_weight, down_weight):
    ep_index = lax.axis_index("ep")
    tp_count = lax.axis_size("tp")
    tp_index = lax.axis_index("tp")
    tok_count, model_width = tokens.shape
    blocks, experts, picks_each = chosen.shape
    slice_width = model_width // tp_count
    columns = lax.dynamic_slice_in_dim(tokens, tp_index * slice_width, slice_width, 1)
    outgoing = lax.dynamic_index_in_dim(chosen, ep_index, 0, keepdims=False)
    leaving = jnp.take(columns, outgoing.reshape(-1), axis=0).reshape(
        experts, picks_each, slice_width
    )
    arrived = lax.all_to_all(leaving, "ep", split_axis=0, concat_axis=0, tiled=True).reshape(
        blocks * picks_each, slice_width
    )
    gate_local = gate_weight[0]
    up_local = up_weight[0]
    portion = gathered_copies(arrived, "tp", 1)
    gate_sum = jnp.dot(portion, gate_local, preferred_element_type=jnp.float32)
    up_sum = jnp.dot(portion, up_local, preferred_element_type=jnp.float32)
    hidden = (jax.nn.silu(gate_sum) * up_sum).astype(jnp.bfloat16)
    down_local = down_weight[0].reshape(down_weight.shape[1], tp_count, slice_width)
    summed = sent_and_summed(
        jnp.einsum("rf,fcd->crd", hidden, down_local, preferred_element_type=jnp.float32).astype(
            jnp.bfloat16
        ),
        "tp",
        0,
    )
    expert_out = summed[0].astype(jnp.bfloat16).reshape(blocks, picks_each, slice_width)
    returned = lax.all_to_all(expert_out, "ep", split_axis=0, concat_axis=0, tiled=True).reshape(
        experts * picks_each, slice_width
    )
    positions = jnp.arange(tok_count, dtype=jnp.int32)[:, None]
    placement_matrix = jnp.where(
        outgoing.reshape(1, -1) == positions, chosen_weight[0].reshape(1, -1), 0.0
    )
    combined = jnp.dot(
        placement_matrix,
        returned.astype(jnp.float32),
        precision=lax.Precision.HIGHEST,
        preferred_element_type=jnp.float32,
    )
    return combined.astype(jnp.bfloat16)


def solution(mesh):
    return jax.shard_map(
        local,
        mesh=mesh,
        in_specs=(
            P("ep", None),
            P(),
            P("ep", None, None),
            P("ep", None, "tp"),
            P("ep", None, "tp"),
            P("ep", "tp", None),
        ),
        out_specs=P("ep", "tp"),
        check_vma=False,
    )
```

profile of v0, /device:TPU:1, one launch (start us, length us, event | category | flops | bytes accessed | tf_op | source)
XLA Modules:
  0.0 183.1 jit_solution(7989967123361729708)
XLA Ops:
  0.0 0.0 copy-start
  0.0 0.8 compare_and_fusion
  0.8 0.1 copy.22
  0.9 0.1 copy.20
  1.0 0.1 reshape.66
  1.1 0.8 constant_dynamic-slice_fusion
  1.9 1.3 gather_fusion
  3.2 0.1 bitcast_select_fusion
  3.3 60.9 %all_to_all.20 = bf16[64,8,128]{2,1,0:T(8,128)(2,1)S(1)} all-to-all(bf16[64,8,128]{2,1,0:T(8,128)(2,1)S(1)} %bitcast_select_fusion), channel_id=1, replica_groups=mesh['ep'=64,'tp'=16] {'ep'}, dimensions={0} | all-to-all | bytes 262144 | tf_op jit(solution)/shard_map/all_to_all | solution.py:47
  64.2 0.1 copy.24
  64.3 1.5 broadcast_in_dim.33
  65.9 6.8 %all-to-all-start.1 = ((bf16[16,512,128]{1,2,0:T(8,128)(2,1)}), bf16[16,512,128]{1,2,0:T(8,128)(2,1)S(1)}, u32[]{:S(2)}, u32[]{:S(2)}) async-start(bf16[16,512,128]{1,2,0:T(8,128)(2,1)} %broadcast_in_dim.33), calls=%async_computation.1 | async-start | bytes 4194304 | tf_op jit(solution)/shard_map/all_to_all | solution.py:9
  72.6 2.5 %copy.27 = bf16[32,8,16,128]{3,2,1,0:T(8,128)(2,1)} copy(bf16[32,8,16,128]{3,1,2,0:T(8,128)(2,1)} %bitcast.40) | data formatting | bytes 2097152
  75.1 26.1 %all-to-all-done.1 = bf16[16,512,128]{1,2,0:T(8,128)(2,1)S(1)} async-done(((bf16[16,512,128]{1,2,0:T(8,128)(2,1)}), bf16[16,512,128]{1,2,0:T(8,128)(2,1)S(1)}, u32[]{:S(2)}, u32[]{:S(2)}) %all-to-all-start.1) | async-done | bytes 2097184 | tf_op jit(solution)/shard_map/all_to_all | solution.py:9
  101.2 2.8 %fusion.3 = f32[512,256]{1,0:T(8,128)} fusion(bf16[512,2048]{0,1:T(8,128)(2,1)S(1)} %bitcast.38, bf16[1,2048,256]{2,1,0:T(8,128)(2,1)} %param.9), kind=kOutput, calls=%fused_computation.7 | convolution fusion | flops 536870912 | bytes 3670016 | tf_op jit(solution)/shard_map/dot_general | solution.py:53
  103.9 5.0 %convert_bitcast_fusion = bf16[16,1,512,128]{3,2,1,0:T(8,128)(2,1)} fusion(bf16[256,16,128]{2,1,0:T(8,128)(2,1)} %bitcast.41, bf16[512,2048]{0,1:T(8,128)(2,1)S(1)} %bitcast.39, bf16[1,2048,256]{2,1,0:T(8,128)(2,1)S(1)} %copy-done, f32[512,256]{1,0:T(8,128)} %fusion.3), kind=kOutput, calls=%fused_computation.1 | convolution fusion | flops 1075576832 | bytes 6815744 | tf_op jit(solution)/shard_map/rf,fcd->crd/dot_general | solution.py:58
  109.0 32.7 %all_to_all.21 = bf16[16,1,512,128]{3,2,1,0:T(8,128)(2,1)S(1)} all-to-all(bf16[16,1,512,128]{3,2,1,0:T(8,128)(2,1)} %convert_bitcast_fusion), channel_id=1, replica_groups=mesh['ep'=64,'tp'=16] {'tp'}, dimensions={0} | all-to-all | bytes 4194304 | tf_op jit(solution)/shard_map/all_to_all | solution.py:31
  141.6 1.0 reduce_sum.12
  142.6 8.9 %all-to-all-start.3 = ((bf16[64,8,128]{2,1,0:T(8,128)(2,1)}), bf16[64,8,128]{2,1,0:T(8,128)(2,1)S(1)}, u32[]{:S(2)}, u32[]{:S(2)}) async-start(bf16[64,8,128]{2,1,0:T(8,128)(2,1)} %bitcast.13), calls=%async_computation.3 | async-start | bytes 262144 | tf_op jit(solution)/shard_map/all_to_all | solution.py:65
  151.5 0.1 eq.17
  151.6 0.1 copy.21
  151.7 0.1 broadcast_in_dim.28
  151.8 30.4 %all-to-all-done.3 = bf16[64,8,128]{2,1,0:T(8,128)(2,1)S(1)} async-done(((bf16[64,8,128]{2,1,0:T(8,128)(2,1)}), bf16[64,8,128]{2,1,0:T(8,128)(2,1)S(1)}, u32[]{:S(2)}, u32[]{:S(2)}) %all-to-all-start.3) | async-done | bytes 131104 | tf_op jit(solution)/shard_map/all_to_all | solution.py:65
  182.2 0.9 convolution_convert_fusion
  (5 shorter events, 0.0 us)
Async XLA Ops:
  0.0 103.9 %copy-start = (bf16[1,2048,256]{2,1,0:T(8,128)(2,1)S(1)}, bf16[1,2048,256]{2,1,0:T(8,128)(2,1)}, u32[]{:S(2)}) copy-start(bf16[1,2048,256]{2,1,0:T(8,128)(2,1)} %param.10) | copy-start | bytes 3145732
  65.9 35.3 %all-to-all-start.1 = ((bf16[16,512,128]{1,2,0:T(8,128)(2,1)}), bf16[16,512,128]{1,2,0:T(8,128)(2,1)S(1)}, u32[]{:S(2)}, u32[]{:S(2)}) async-start(bf16[16,512,128]{1,2,0:T(8,128)(2,1)} %broadcast_in_dim.33), calls=%async_computation.1 | async-start | bytes 4194304 | tf_op jit(solution)/shard_map/all_to_all | solution.py:9
  141.6 10.0 %copy-start.1 = (f32[1,64,8]{1,2,0:T(8,128)S(1)}, f32[1,64,8]{1,2,0:T(8,128)}, u32[]{:S(2)}) copy-start(f32[1,64,8]{1,2,0:T(8,128)} %param.8) | copy-start | bytes 6148
  142.6 39.6 %all-to-all-start.3 = ((bf16[64,8,128]{2,1,0:T(8,128)(2,1)}), bf16[64,8,128]{2,1,0:T(8,128)(2,1)S(1)}, u32[]{:S(2)}, u32[]{:S(2)}) async-start(bf16[64,8,128]{2,1,0:T(8,128)(2,1)} %bitcast.13), calls=%async_computation.3 | async-start | bytes 262144 | tf_op jit(solution)/shard_map/all_to_all | solution.py:65
where the time goes:
time: 184 us; the launch traced here: 183 us
  blocking collectives  93.5 us (51%)
  waiting for transfers between devices  56.5 us (31%)
  starting transfers between devices  15.7 us (9%)
  matrix products  8.69 us (5%)
  local copies, waits for them, and re-layouts  6.76 us (4%)
  other arithmetic  1.89 us (1%)
    all_to_all x1, blocking collectives, local(): lax.all_to_all(leaving, 'ep', split_axis=0, concat_axis=0, tiled=True)  60.9 us
    all_to_all x1, blocking collectives, sent_and_summed(): lax.all_to_all(tiles, axis, split_axis=0, concat_axis=0, tiled=True)  32.7 us
    all_to_all x1, waiting for transfers between devices, local(): lax.all_to_all(expert_out, 'ep', split_axis=0, concat_axis=0, tiled=True)  30.4 us
    all_to_all x1, waiting for transfers between devices, from_everyone(): return lax.all_to_all(copies, axis, split_axis=0, concat_axis=0, tiled=True)  26.1 us
    all_to_all x1, starting transfers between devices, local(): lax.all_to_all(expert_out, 'ep', split_axis=0, concat_axis=0, tiled=True)  8.93 us
    all_to_all x1, starting transfers between devices, from_everyone(): return lax.all_to_all(copies, axis, split_axis=0, concat_axis=0, tiled=True)  6.75 us
    dot_general x1, matrix products, local(): jnp.einsum('rf,fcd->crd', hidden, down_local, preferred_element_type=jnp....  5.05 us
  transfers between devices with their start and end apart: 2, of which 2 were waited for; matrix products, arithmetic and copies ran while one was open for 1% of the time, Pallas kernels for 0%

commit v1 on v0

v1 whole, which is shorter than its diff:
```python
import functools

import jax
import jax.numpy as jnp
from jax import lax
from jax.experimental import pallas as pl
from jax.experimental.pallas import tpu as pltpu
from jax.sharding import PartitionSpec as P

GRID = 4
STEPS = ((0, 1), (0, -1), (1, 0), (-1, 0))
VMEM = pl.BlockSpec(memory_space=pltpu.VMEM)
HBM = pl.BlockSpec(memory_space=pltpu.HBM)


def colour(u):
    return (u // GRID + u % GRID) % 2


def neighbour_pairs(dy, dx):
    return [
        (y * GRID + x, (y + dy) % GRID * GRID + (x + dx) % GRID)
        for y in range(GRID)
        for x in range(GRID)
    ]


def cost(flops, nbytes):
    return pl.CostEstimate(flops=flops, bytes_accessed=nbytes, transcendentals=0)


def in_hbm(array):
    return pltpu.with_memory_space_constraint(array, pltpu.HBM)


def room(mib):
    return pltpu.CompilerParams(vmem_limit_bytes=mib * 2**20)


def pick_kernel(tokens, chosen, out, columns, picks, sems):
    width = out.shape[1]
    start = pl.multiple_of(lax.axis_index("tp") * width, width)
    get_columns = pltpu.make_async_copy(tokens.at[:, pl.ds(start, width)], columns, sems.at[0])
    get_picks = pltpu.make_async_copy(chosen.at[lax.axis_index("ep")], picks, sems.at[1])
    get_columns.start()
    get_picks.start()
    rows = out.shape[0]
    each, experts = picks.shape
    row = lax.broadcasted_iota(jnp.int32, (rows, experts), 0)
    expert = lax.broadcasted_iota(jnp.int32, (rows, experts), 1)
    spread = jnp.where(row // each == expert, 1.0, 0.0).astype(jnp.bfloat16)
    row = lax.broadcasted_iota(jnp.int32, (rows, each), 0)
    pick = lax.broadcasted_iota(jnp.int32, (rows, each), 1)
    mine = row % each == pick
    ones = jnp.ones((each, columns.shape[0]), jnp.bfloat16)
    place = lax.broadcasted_iota(jnp.int32, (rows, columns.shape[0]), 1)
    get_picks.wait()
    all_picks = lax.dot_general(
        spread,
        picks[...].astype(jnp.float32).astype(jnp.bfloat16),
        (((1,), (1,)), ((), ())),
        preferred_element_type=jnp.float32,
    )
    own = jnp.where(mine, all_picks, 0.0).astype(jnp.bfloat16)
    position = jnp.dot(own, ones, preferred_element_type=jnp.float32)
    one_hot = jnp.where(position.astype(jnp.int32) == place, 1.0, 0.0).astype(jnp.bfloat16)
    get_columns.wait()
    out[...] = jnp.dot(one_hot, columns[...], preferred_element_type=jnp.float32).astype(out.dtype)


def place_kernel(chosen, weight, out, picks, sem):
    get_picks = pltpu.make_async_copy(chosen.at[lax.axis_index("ep")], picks, sem)
    get_picks.start()
    each, experts = picks.shape
    tok_count, rows = out.shape[1:]
    row = lax.broadcasted_iota(jnp.int32, (experts, rows), 1)
    expert = lax.broadcasted_iota(jnp.int32, (experts, rows), 0)
    spread = jnp.where(row // each == expert, 1.0, 0.0).astype(jnp.bfloat16)
    row = lax.broadcasted_iota(jnp.int32, (each, rows), 1)
    pick = lax.broadcasted_iota(jnp.int32, (each, rows), 0)
    mine = row % each == pick
    place = lax.broadcasted_iota(jnp.int32, (tok_count, rows), 0)

    def in_row(values):
        every = jnp.dot(values.astype(jnp.bfloat16), spread, preferred_element_type=jnp.float32)
        return jnp.sum(jnp.where(mine, every, 0.0), axis=0, keepdims=True)

    rest = weight[...]
    get_picks.wait()
    here = in_row(picks[...].astype(jnp.float32)).astype(jnp.int32) == place
    for k in range(3):
        term = rest.astype(jnp.bfloat16)
        rest = rest - term.astype(jnp.float32)
        out[k] = jnp.where(here, in_row(term), 0.0).astype(out.dtype)


def combine_kernel(places, rows, out):
    total = jnp.dot(places[0], rows[...], preferred_element_type=jnp.float32)
    for k in range(1, places.shape[0]):
        total += jnp.dot(places[k], rows[...], preferred_element_type=jnp.float32)
    out[...] = total.astype(out.dtype)


def pack_kernel(gate, up, down, *outs):
    depth, units = gate.shape
    part = units // len(outs)
    lanes = 2 * part
    for q, out in enumerate(outs):
        g = gate[:, q * part : (q + 1) * part]
        u = up[:, q * part : (q + 1) * part]
        out[:depth, :] = jnp.concatenate([g, u] if q % 2 == 0 else [u, g], axis=1)
        for c in range(down.shape[1] // lanes):
            out[depth + c * part : depth + (c + 1) * part, :] = down[
                q * part : (q + 1) * part, c * lanes : (c + 1) * lanes
            ]


def spread_kernel(rows, out):
    half = out.shape[1]
    for u in range(out.shape[0]):
        out[u] = rows[colour(u) * half : (colour(u) + 1) * half, :]


def silu(v):
    return v / (1.0 + jnp.exp(-v))


def ffn_kernel(tiles, gate, up, down, p0, p1, p2, p3, out, rows):
    chunks, count, lanes = tiles.shape
    depth, units = gate.shape
    part = units // 4
    for t in range(chunks):
        rows[:, t * lanes : (t + 1) * lanes] = tiles[t]
    low = lax.broadcasted_iota(jnp.int32, (count, lanes), 1) < part
    gate_sum = jnp.dot(rows[...], gate[...], preferred_element_type=jnp.float32)
    up_sum = jnp.dot(rows[...], up[...], preferred_element_type=jnp.float32)
    hidden = [(silu(gate_sum) * up_sum).astype(jnp.bfloat16)]
    for a, b in ((p0, p1), (p2, p3)):
        both = jnp.dot(
            rows[...],
            jnp.concatenate([a[:depth, :], b[:depth, :]], axis=1),
            preferred_element_type=jnp.float32,
        )
        left, right = both[:, :lanes], both[:, lanes:]
        left = silu(left) * pltpu.roll(left, part, 1)
        right = silu(right) * pltpu.roll(right, part, 1)
        hidden.append(jnp.where(low, left, right).astype(jnp.bfloat16))
    hidden = jnp.concatenate(hidden, axis=1)
    for c in range(0, chunks, 2):
        theirs = [
            jnp.concatenate(
                [p[depth + k * part : depth + (k + 1) * part, :] for p in (p0, p1, p2, p3)], axis=0
            )
            for k in (c, c + 1)
        ]
        weights = jnp.concatenate(
            [down[:, c * lanes : (c + 2) * lanes], jnp.concatenate(theirs, axis=1)], axis=0
        )
        sums = jnp.dot(hidden, weights, preferred_element_type=jnp.float32).astype(out.dtype)
        out[c] = sums[:, :lanes]
        out[c + 1] = sums[:, lanes:]


def sum_kernel(parts, out):
    half = parts.shape[1]
    for k in range(2):
        total = None
        for u in range(parts.shape[0]):
            if colour(u) == k:
                term = parts[u].astype(jnp.float32)
                total = term if total is None else total + term
        out[k * half : (k + 1) * half, :] = total.astype(out.dtype)


def exchange(tiles, axis):
    return lax.all_to_all(tiles, axis, split_axis=0, concat_axis=0, tiled=True)


def local(tokens, chosen, chosen_weight, gate_weight, up_weight, down_weight):
    tp_count = lax.axis_size("tp")
    tok_count, model_width = tokens.shape
    blocks, experts, picks_each = chosen.shape
    width = model_width // tp_count
    count = blocks * picks_each
    gate, up, down = gate_weight[0], up_weight[0], down_weight[0]
    units = gate.shape[1]
    bf16 = functools.partial(jax.ShapeDtypeStruct, dtype=jnp.bfloat16)

    by_pick = in_hbm(jnp.transpose(chosen, (0, 2, 1)))
    leaving = pl.pallas_call(
        pick_kernel,
        out_shape=bf16((count, width)),
        in_specs=[HBM, HBM],
        out_specs=VMEM,
        scratch_shapes=[
            pltpu.VMEM((tok_count, width), jnp.bfloat16),
            pltpu.VMEM((picks_each, experts), jnp.int32),
            pltpu.SemaphoreType.DMA((2,)),
        ],
        compiler_params=room(4),
        cost_estimate=cost(2 * count * tok_count * width, 4 * count * width),
        name="pick",
    )(in_hbm(tokens), by_pick)
    arrived = exchange(leaving.reshape(experts, picks_each, width), "ep").reshape(count, width)

    pack = pl.pallas_call(
        pack_kernel,
        out_shape=[bf16((model_width + model_width // 2, units // 2))] * 4,
        in_specs=[VMEM] * 3,
        out_specs=[VMEM] * 4,
        compiler_params=room(12),
        cost_estimate=cost(10**8, 12 * model_width * units),
        name="pack",
    )
    packs = pack(gate, up, down)
    shared = [
        lax.ppermute(pack, "tp", neighbour_pairs(*step))
        for pack, step in zip(packs, STEPS, strict=True)
    ]

    place = pl.pallas_call(
        place_kernel,
        out_shape=bf16((3, tok_count, count)),
        in_specs=[HBM, VMEM],
        out_specs=VMEM,
        scratch_shapes=[pltpu.VMEM((picks_each, experts), jnp.int32), pltpu.SemaphoreType.DMA],
        compiler_params=room(4),
        cost_estimate=cost(10**8, 8 * tok_count * count),
        name="place",
    )
    places = place(by_pick, jnp.transpose(chosen_weight[0]))

    tiles = pl.pallas_call(
        spread_kernel,
        out_shape=bf16((tp_count, count // 2, width)),
        in_specs=[VMEM],
        out_specs=VMEM,
        compiler_params=room(6),
        cost_estimate=cost(10**8, tp_count * count * width),
        name="spread",
    )(arrived)
    tiles = exchange(tiles, "tp")
    partial = pl.pallas_call(
        ffn_kernel,
        out_shape=bf16((tp_count, count // 2, width)),
        in_specs=[VMEM] * 8,
        out_specs=VMEM,
        scratch_shapes=[pltpu.VMEM((count // 2, model_width), jnp.bfloat16)],
        cost_estimate=cost(6 * count * model_width * units, 12 * model_width * units),
        compiler_params=room(20),
        name="ffn",
    )(tiles, gate, up, down, *shared)
    partial = exchange(partial, "tp")
    expert_out = pl.pallas_call(
        sum_kernel,
        out_shape=bf16((count, width)),
        in_specs=[VMEM],
        out_specs=VMEM,
        compiler_params=room(6),
        cost_estimate=cost(10**8, tp_count * count * width),
        name="add",
    )(partial)
    returned = exchange(expert_out.reshape(blocks, picks_each, width), "ep").reshape(
        experts * picks_each, width
    )
    return pl.pallas_call(
        combine_kernel,
        out_shape=bf16((tok_count, width)),
        in_specs=[VMEM] * 2,
        out_specs=VMEM,
        compiler_params=room(4),
        cost_estimate=cost(6 * tok_count * count * width, 8 * tok_count * count),
        name="combine",
    )(places, returned)


def solution(mesh):
    return jax.shard_map(
        local,
        mesh=mesh,
        in_specs=(
            P("ep", None),
            P(),
            P("ep", None, None),
            P("ep", None, "tp"),
            P("ep", None, "tp"),
            P("ep", "tp", None),
        ),
        out_specs=P("ep", "tp"),
        check_vma=False,
    )
```

time: 184 us -> 175 us (0.951)
  blocking collectives: 93.5 us -> 81.8 us
  starting transfers between devices: 15.7 us -> 27.4 us
  waiting for transfers between devices: 56.5 us -> 47.6 us
  Pallas kernels: 0 us -> 8.88 us
  matrix products: 8.69 us -> 0 us
  other arithmetic: 1.89 us -> 0 us
    all_to_all x2, waiting for transfers between devices: 56.5 us -> 29.7 us  [exchange(): return lax.all_to_all(tiles, axis, split_axis=0, concat_axis=0, tiled=True)]
    ppermute x0 -> x4, waiting for transfers between devices: none -> 17.9 us  [local(): lax.ppermute(pack, 'tp', neighbour_pairs(*step))]
    ppermute x0 -> x4, starting transfers between devices: none -> 13 us  [local(): lax.ppermute(pack, 'tp', neighbour_pairs(*step))]
    all_to_all x2, blocking collectives: 93.5 us -> 81.8 us  [exchange(): return lax.all_to_all(tiles, axis, split_axis=0, concat_axis=0, tiled=True)]
    pallas_call x0 -> x7, Pallas kernels: none -> 8.88 us  [the longest x1 3.17 us: local(): pl.pallas_call(ffn_kernel, out_shape=bf16((tp_count, count // 2, width)),...]
    dot_general x3 -> x0, matrix products: 8.69 us -> none  [the longest x1 5.05 us: local(): jnp.einsum('rf,fcd->crd', hidden, down_local, preferred_element_type=jnp....]
    unnamed x6 -> x24, local copies, waits for them, and re-layouts: 2.55 us -> 8.1 us
  transfers between devices with their start and end apart: 2 -> 6, of which waited for: 2 -> 2; matrix products, arithmetic and copies ran while one was open for 1% -> 0% of each run, Pallas kernels for 0% -> 1%
where the time goes in v1:
time: 175 us; the launch traced here: 174 us
  blocking collectives  81.8 us (47%)
  waiting for transfers between devices  47.6 us (27%)
  starting transfers between devices  27.4 us (16%)
  Pallas kernels  8.88 us (5%)
  local copies, waits for them, and re-layouts  8.1 us (5%)
    all_to_all x2, blocking collectives, exchange(): return lax.all_to_all(tiles, axis, split_axis=0, concat_axis=0, tiled=True)  81.8 us
    all_to_all x2, waiting for transfers between devices, exchange(): return lax.all_to_all(tiles, axis, split_axis=0, concat_axis=0, tiled=True)  29.7 us
    ppermute x4, waiting for transfers between devices, local(): lax.ppermute(pack, 'tp', neighbour_pairs(*step))  17.9 us
    all_to_all x2, starting transfers between devices, exchange(): return lax.all_to_all(tiles, axis, split_axis=0, concat_axis=0, tiled=True)  14.4 us
    ppermute x4, starting transfers between devices, local(): lax.ppermute(pack, 'tp', neighbour_pairs(*step))  13 us
    unnamed x24, local copies, waits for them, and re-layouts  8.1 us
  transfers between devices with their start and end apart: 6, of which 2 were waited for; matrix products, arithmetic and copies ran while one was open for 0% of the time, Pallas kernels for 1%

profile of v1, /device:TPU:1, one launch (start us, length us, event | category | flops | bytes accessed | tf_op | source)
XLA Modules:
  0.0 173.9 jit_solution(804276028463608106)
XLA Ops:
  0.0 1.2 pick.1
  1.2 60.9 %all_to_all.20 = bf16[64,8,128]{2,1,0:T(8,128)(2,1)S(1)} all-to-all(bf16[64,8,128]{2,1,0:T(8,128)(2,1)S(1)} %bitcast.19), channel_id=1, replica_groups=mesh['ep'=64,'tp'=16] {'ep'}, dimensions={0} | all-to-all | bytes 262144 | tf_op jit(solution)/shard_map/all_to_all | solution.py:176
  62.1 1.1 spread.1
  63.2 7.0 %all-to-all-start.1 = ((bf16[16,256,128]{2,1,0:T(8,128)(2,1)}), bf16[16,256,128]{2,1,0:T(8,128)(2,1)}, u32[]{:S(2)}, u32[]{:S(2)}) async-start(bf16[16,256,128]{2,1,0:T(8,128)(2,1)} %spread.1), calls=%async_computation.1 | async-start | bytes 2097152 | tf_op jit(solution)/shard_map/all_to_all | solution.py:176
  71.0 3.2 %collective-permute-start = (bf16[3072,128]{1,0:T(8,128)(2,1)S(1)}, bf16[3072,128]{1,0:T(8,128)(2,1)S(1)}, u32[]{:S(2)}, u32[]{:S(2)}) collective-permute-start(bf16[3072,128]{1,0:T(8,128)(2,1)S(1)} %get-tuple-element.9), channel_id=1, source_target_pairs={{0,1},{1,2},{2,3},{3,0},{4,5},{5,6},{6,7},{7,4},{8,9},{9,10},{10,1... | collective-permute-start | bytes 2359304 | tf_op jit(solution)/shard_map/ppermute | solution.py:217
  74.2 3.3 %collective-permute-start.1 = (bf16[3072,128]{1,0:T(8,128)(2,1)S(1)}, bf16[3072,128]{1,0:T(8,128)(2,1)S(1)}, u32[]{:S(2)}, u32[]{:S(2)}) collective-permute-start(bf16[3072,128]{1,0:T(8,128)(2,1)S(1)} %get-tuple-element.10), channel_id=1, source_target_pairs={{0,3},{1,0},{2,1},{3,2},{4,7},{5,4},{6,5},{7,6},{8,11},{9,8},{10,9... | collective-permute-start | bytes 2359304 | tf_op jit(solution)/shard_map/ppermute | solution.py:217
  77.5 3.2 %collective-permute-start.2 = (bf16[3072,128]{1,0:T(8,128)(2,1)S(1)}, bf16[3072,128]{1,0:T(8,128)(2,1)S(1)}, u32[]{:S(2)}, u32[]{:S(2)}) collective-permute-start(bf16[3072,128]{1,0:T(8,128)(2,1)S(1)} %get-tuple-element.11), channel_id=1, source_target_pairs={{0,4},{1,5},{2,6},{3,7},{4,8},{5,9},{6,10},{7,11},{8,12},{9,13},{1... | collective-permute-start | bytes 2359304 | tf_op jit(solution)/shard_map/ppermute | solution.py:217
  80.7 3.3 %collective-permute-start.3 = (bf16[3072,128]{1,0:T(8,128)(2,1)S(1)}, bf16[3072,128]{1,0:T(8,128)(2,1)S(1)}, u32[]{:S(2)}, u32[]{:S(2)}) collective-permute-start(bf16[3072,128]{1,0:T(8,128)(2,1)S(1)} %get-tuple-element.12), channel_id=1, source_target_pairs={{0,12},{1,13},{2,14},{3,15},{4,0},{5,1},{6,2},{7,3},{8,4},{9,5},{1... | collective-permute-start | bytes 2359304 | tf_op jit(solution)/shard_map/ppermute | solution.py:217
  84.0 17.9 %collective-permute-done.p0 = bf16[3072,128]{1,0:T(8,128)(2,1)S(1)} collective-permute-done((bf16[3072,128]{1,0:T(8,128)(2,1)S(1)}, bf16[3072,128]{1,0:T(8,128)(2,1)S(1)}, u32[]{:S(2)}, u32[]{:S(2)}) %collective-permute-start) | collective-permute-done | bytes 786464 | tf_op jit(solution)/shard_map/ppermute | solution.py:217
  101.9 0.9 copy-done.3
  102.8 0.9 copy-done.5
  103.6 0.9 copy-done.7
  104.5 0.9 copy-done.9
  105.4 1.1 copy-done.4
  106.6 1.1 copy-done.6
  107.7 1.1 copy-done.8
  108.8 1.1 copy-done.10
  110.0 3.2 %ffn.1 = bf16[16,256,128]{2,1,0:T(8,128)(2,1)S(1)} custom-call(bf16[16,256,128]{2,1,0:T(8,128)(2,1)} %all-to-all-done.1.tiles, bf16[2048,256]{1,0:T(8,128)(2,1)S(1)} %bitcast.12, bf16[2048,256]{1,0:T(8,128)(2,1)S(1)} %bitcast.14, bf16[256,2048]{1,0:T(8,128)(2,1)S(1)} %bitcast.16, bf16[3072,128]{1,0:T(8,128)(2,1)S(1)} %copy-done.4, ...), custom_call_target="tpu_custom_call" | custom-call | flops 1610612736 | bytes 6291456 | tf_op jit(solution)/shard_map/ffn/pallas_call | solution.py:243
  113.2 20.9 %all_to_all.21.parts = bf16[16,256,128]{2,1,0:T(8,128)(2,1)S(1)} all-to-all(bf16[16,256,128]{2,1,0:T(8,128)(2,1)S(1)} %ffn.1), channel_id=1, replica_groups=mesh['ep'=64,'tp'=16] {'tp'}, dimensions={0} | all-to-all | bytes 2097152 | tf_op jit(solution)/shard_map/all_to_all | solution.py:176
  134.1 0.8 add.1
  134.9 7.5 %all-to-all-start.3 = ((bf16[64,8,128]{2,1,0:T(8,128)(2,1)}), bf16[64,8,128]{2,1,0:T(8,128)(2,1)S(1)}, u32[]{:S(2)}, u32[]{:S(2)}) async-start(bf16[64,8,128]{2,1,0:T(8,128)(2,1)} %bitcast.8), calls=%async_computation.3 | async-start | bytes 262144 | tf_op jit(solution)/shard_map/all_to_all | solution.py:176
  142.4 0.9 place.1.places
  143.3 29.7 %all-to-all-done.3 = bf16[64,8,128]{2,1,0:T(8,128)(2,1)S(1)} async-done(((bf16[64,8,128]{2,1,0:T(8,128)(2,1)}), bf16[64,8,128]{2,1,0:T(8,128)(2,1)S(1)}, u32[]{:S(2)}, u32[]{:S(2)}) %all-to-all-start.3) | async-done | bytes 131104 | tf_op jit(solution)/shard_map/all_to_all | solution.py:176
  173.0 0.9 combine.1
  (21 shorter events, 0.8 us)
Async XLA Ops:
  62.1 8.1 %copy-start.2 = (bf16[1,256,2048]{2,1,0:T(8,128)(2,1)S(1)}, bf16[1,256,2048]{2,1,0:T(8,128)(2,1)}, u32[]{:S(2)}) copy-start(bf16[1,256,2048]{2,1,0:T(8,128)(2,1)} %param.11) | copy-start | bytes 3145732
  63.2 7.0 %copy-start = (bf16[1,2048,256]{2,1,0:T(8,128)(2,1)S(1)}, bf16[1,2048,256]{2,1,0:T(8,128)(2,1)}, u32[]{:S(2)}) copy-start(bf16[1,2048,256]{2,1,0:T(8,128)(2,1)} %param.9) | copy-start | bytes 3145732
  63.2 7.0 %copy-start.1 = (bf16[1,2048,256]{2,1,0:T(8,128)(2,1)S(1)}, bf16[1,2048,256]{2,1,0:T(8,128)(2,1)}, u32[]{:S(2)}) copy-start(bf16[1,2048,256]{2,1,0:T(8,128)(2,1)} %param.10) | copy-start | bytes 3145732
  63.2 42.2 %all-to-all-start.1 = ((bf16[16,256,128]{2,1,0:T(8,128)(2,1)}), bf16[16,256,128]{2,1,0:T(8,128)(2,1)}, u32[]{:S(2)}, u32[]{:S(2)}) async-start(bf16[16,256,128]{2,1,0:T(8,128)(2,1)} %spread.1), calls=%async_computation.1 | async-start | bytes 2097152 | tf_op jit(solution)/shard_map/all_to_all | solution.py:176
  71.0 30.9 %collective-permute-start = (bf16[3072,128]{1,0:T(8,128)(2,1)S(1)}, bf16[3072,128]{1,0:T(8,128)(2,1)S(1)}, u32[]{:S(2)}, u32[]{:S(2)}) collective-permute-start(bf16[3072,128]{1,0:T(8,128)(2,1)S(1)} %get-tuple-element.9), channel_id=1, source_target_pairs={{0,1},{1,2},{2,3},{3,0},{4,5},{5,6},{6,7},{7,4},{8,9},{9,10},{10,1... | collective-permute-start | bytes 2359304 | tf_op jit(solution)/shard_map/ppermute | solution.py:217
  74.2 28.6 %collective-permute-start.1 = (bf16[3072,128]{1,0:T(8,128)(2,1)S(1)}, bf16[3072,128]{1,0:T(8,128)(2,1)S(1)}, u32[]{:S(2)}, u32[]{:S(2)}) collective-permute-start(bf16[3072,128]{1,0:T(8,128)(2,1)S(1)} %get-tuple-element.10), channel_id=1, source_target_pairs={{0,3},{1,0},{2,1},{3,2},{4,7},{5,4},{6,5},{7,6},{8,11},{9,8},{10,9... | collective-permute-start | bytes 2359304 | tf_op jit(solution)/shard_map/ppermute | solution.py:217
  77.5 26.1 %collective-permute-start.2 = (bf16[3072,128]{1,0:T(8,128)(2,1)S(1)}, bf16[3072,128]{1,0:T(8,128)(2,1)S(1)}, u32[]{:S(2)}, u32[]{:S(2)}) collective-permute-start(bf16[3072,128]{1,0:T(8,128)(2,1)S(1)} %get-tuple-element.11), channel_id=1, source_target_pairs={{0,4},{1,5},{2,6},{3,7},{4,8},{5,9},{6,10},{7,11},{8,12},{9,13},{1... | collective-permute-start | bytes 2359304 | tf_op jit(solution)/shard_map/ppermute | solution.py:217
  80.7 23.8 %collective-permute-start.3 = (bf16[3072,128]{1,0:T(8,128)(2,1)S(1)}, bf16[3072,128]{1,0:T(8,128)(2,1)S(1)}, u32[]{:S(2)}, u32[]{:S(2)}) collective-permute-start(bf16[3072,128]{1,0:T(8,128)(2,1)S(1)} %get-tuple-element.12), channel_id=1, source_target_pairs={{0,12},{1,13},{2,14},{3,15},{4,0},{5,1},{6,2},{7,3},{8,4},{9,5},{1... | collective-permute-start | bytes 2359304 | tf_op jit(solution)/shard_map/ppermute | solution.py:217
  101.9 0.9 copy-start.3
  102.8 0.9 copy-start.5
  103.6 0.9 copy-start.7
  104.5 0.9 copy-start.9
  105.4 1.1 copy-start.4
  106.6 1.1 copy-start.6
  107.7 1.1 copy-start.8
  108.8 1.1 copy-start.10
  134.9 7.5 %copy-start.11 = (f32[1,64,8]{1,2,0:T(8,128)S(1)}, f32[1,64,8]{1,2,0:T(8,128)}, u32[]{:S(2)}) copy-start(f32[1,64,8]{1,2,0:T(8,128)} %param.8) | copy-start | bytes 6148
  134.9 38.2 %all-to-all-start.3 = ((bf16[64,8,128]{2,1,0:T(8,128)(2,1)}), bf16[64,8,128]{2,1,0:T(8,128)(2,1)S(1)}, u32[]{:S(2)}, u32[]{:S(2)}) async-start(bf16[64,8,128]{2,1,0:T(8,128)(2,1)} %bitcast.8), calls=%async_computation.3 | async-start | bytes 262144 | tf_op jit(solution)/shard_map/all_to_all | solution.py:176

commit v2 on v1

--- a/solution.py
+++ b/solution.py
@@ -48,7 +48,8 @@
     each, experts = picks.shape
     row = lax.broadcasted_iota(jnp.int32, (rows, experts), 0)
     expert = lax.broadcasted_iota(jnp.int32, (rows, experts), 1)
-    spread = jnp.where(row // each == expert, 1.0, 0.0).astype(jnp.bfloat16)
+    spread = jnp.where((row // each + experts // 2) % experts == expert, 1.0, 0.0)
+    spread = spread.astype(jnp.bfloat16)
     row = lax.broadcasted_iota(jnp.int32, (rows, each), 0)
     pick = lax.broadcasted_iota(jnp.int32, (rows, each), 1)
     mine = row % each == pick
@@ -169,11 +170,15 @@
             if colour(u) == k:
                 term = parts[u].astype(jnp.float32)
                 total = term if total is None else total + term
-        out[k * half : (k + 1) * half, :] = total.astype(out.dtype)
-
-
-def exchange(tiles, axis):
-    return lax.all_to_all(tiles, axis, split_axis=0, concat_axis=0, tiled=True)
+        out[(1 - k) * half : (2 - k) * half, :] = total.astype(out.dtype)
+
+
+def exchange(tiles, axis, first=0):
+    size = lax.axis_size(axis)
+    groups = [[(i + first) % size for i in range(size)]] if first else None
+    return lax.all_to_all(
+        tiles, axis, split_axis=0, concat_axis=0, axis_index_groups=groups, tiled=True
+    )
 
 
 def local(tokens, chosen, chosen_weight, gate_weight, up_weight, down_weight):
@@ -201,7 +206,9 @@
         cost_estimate=cost(2 * count * tok_count * width, 4 * count * width),
         name="pick",
     )(in_hbm(tokens), by_pick)
-    arrived = exchange(leaving.reshape(experts, picks_each, width), "ep").reshape(count, width)
+    arrived = exchange(
+        leaving.reshape(experts, picks_each, width), "ep", experts // 2
+    ).reshape(count, width)
 
     pack = pl.pallas_call(
         pack_kernel,

time: 175 us -> 178 us (1.017)
  starting transfers between devices: 27.4 us -> 41.4 us
  blocking collectives: 81.8 us -> 71.6 us
    all_to_all x2, starting transfers between devices: 14.4 us -> 28.4 us  [exchange(): lax.all_to_all(tiles, axis, split_axis=0, concat_axis=0, axis_index_group...]
    all_to_all x2, blocking collectives: 81.8 us -> 71.6 us  [exchange(): lax.all_to_all(tiles, axis, split_axis=0, concat_axis=0, axis_index_group...]
where the time goes in v2:
time: 178 us
  blocking collectives  71.6 us (40%)
  waiting for transfers between devices  47.6 us (27%)
  starting transfers between devices  41.4 us (23%)
  Pallas kernels  8.87 us (5%)
  local copies, waits for them, and re-layouts  8.1 us (5%)
    all_to_all x2, blocking collectives, exchange(): lax.all_to_all(tiles, axis, split_axis=0, concat_axis=0, axis_index_group...  71.6 us
    all_to_all x2, waiting for transfers between devices, exchange(): lax.all_to_all(tiles, axis, split_axis=0, concat_axis=0, axis_index_group...  29.7 us
    all_to_all x2, starting transfers between devices, exchange(): lax.all_to_all(tiles, axis, split_axis=0, concat_axis=0, axis_index_group...  28.4 us
    ppermute x4, waiting for transfers between devices, local(): lax.ppermute(pack, 'tp', neighbour_pairs(*step))  17.9 us
    ppermute x4, starting transfers between devices, local(): lax.ppermute(pack, 'tp', neighbour_pairs(*step))  13 us
    unnamed x24, local copies, waits for them, and re-layouts  8.1 us
  transfers between devices with their start and end apart: 6, of which 2 were waited for; matrix products, arithmetic and copies ran while one was open for 0% of the time, Pallas kernels for 1%

profile of v2, /device:TPU:1, one launch (start us, length us, event | category | flops | bytes accessed | tf_op | source)
XLA Modules:
  0.0 177.7 jit_solution(14138290237348883634)
XLA Ops:
  0.0 1.2 pick.1
  1.2 49.6 %all_to_all.20 = bf16[64,8,128]{2,1,0:T(8,128)(2,1)S(1)} all-to-all(bf16[64,8,128]{2,1,0:T(8,128)(2,1)S(1)} %bitcast.19), channel_id=1, replica_groups={{512,528,544,560,576,592,608,624,640,656,672,688,704,720,736,752,768,78..., dimensions={0} | all-to-all | bytes 262144 | tf_op jit(solution)/shard_map/all_to_all | solution.py:179
  50.9 1.1 spread.1
  52.0 6.9 %all-to-all-start.1 = ((bf16[16,256,128]{2,1,0:T(8,128)(2,1)}), bf16[16,256,128]{2,1,0:T(8,128)(2,1)}, u32[]{:S(2)}, u32[]{:S(2)}) async-start(bf16[16,256,128]{2,1,0:T(8,128)(2,1)} %spread.1), calls=%async_computation.1 | async-start | bytes 2097152 | tf_op jit(solution)/shard_map/all_to_all | solution.py:179
  59.7 3.2 %collective-permute-start = (bf16[3072,128]{1,0:T(8,128)(2,1)S(1)}, bf16[3072,128]{1,0:T(8,128)(2,1)S(1)}, u32[]{:S(2)}, u32[]{:S(2)}) collective-permute-start(bf16[3072,128]{1,0:T(8,128)(2,1)S(1)} %get-tuple-element.9), channel_id=1, source_target_pairs={{0,1},{1,2},{2,3},{3,0},{4,5},{5,6},{6,7},{7,4},{8,9},{9,10},{10,1... | collective-permute-start | bytes 2359304 | tf_op jit(solution)/shard_map/ppermute | solution.py:224
  63.0 3.3 %collective-permute-start.1 = (bf16[3072,128]{1,0:T(8,128)(2,1)S(1)}, bf16[3072,128]{1,0:T(8,128)(2,1)S(1)}, u32[]{:S(2)}, u32[]{:S(2)}) collective-permute-start(bf16[3072,128]{1,0:T(8,128)(2,1)S(1)} %get-tuple-element.10), channel_id=1, source_target_pairs={{0,3},{1,0},{2,1},{3,2},{4,7},{5,4},{6,5},{7,6},{8,11},{9,8},{10,9... | collective-permute-start | bytes 2359304 | tf_op jit(solution)/shard_map/ppermute | solution.py:224
  66.2 3.2 %collective-permute-start.2 = (bf16[3072,128]{1,0:T(8,128)(2,1)S(1)}, bf16[3072,128]{1,0:T(8,128)(2,1)S(1)}, u32[]{:S(2)}, u32[]{:S(2)}) collective-permute-start(bf16[3072,128]{1,0:T(8,128)(2,1)S(1)} %get-tuple-element.11), channel_id=1, source_target_pairs={{0,4},{1,5},{2,6},{3,7},{4,8},{5,9},{6,10},{7,11},{8,12},{9,13},{1... | collective-permute-start | bytes 2359304 | tf_op jit(solution)/shard_map/ppermute | solution.py:224
  69.5 3.3 %collective-permute-start.3 = (bf16[3072,128]{1,0:T(8,128)(2,1)S(1)}, bf16[3072,128]{1,0:T(8,128)(2,1)S(1)}, u32[]{:S(2)}, u32[]{:S(2)}) collective-permute-start(bf16[3072,128]{1,0:T(8,128)(2,1)S(1)} %get-tuple-element.12), channel_id=1, source_target_pairs={{0,12},{1,13},{2,14},{3,15},{4,0},{5,1},{6,2},{7,3},{8,4},{9,5},{1... | collective-permute-start | bytes 2359304 | tf_op jit(solution)/shard_map/ppermute | solution.py:224
  72.8 17.9 %collective-permute-done.p0 = bf16[3072,128]{1,0:T(8,128)(2,1)S(1)} collective-permute-done((bf16[3072,128]{1,0:T(8,128)(2,1)S(1)}, bf16[3072,128]{1,0:T(8,128)(2,1)S(1)}, u32[]{:S(2)}, u32[]{:S(2)}) %collective-permute-start) | collective-permute-done | bytes 786464 | tf_op jit(solution)/shard_map/ppermute | solution.py:224
  90.6 0.9 copy-done.3
  91.5 0.9 copy-done.5
  92.4 0.9 copy-done.7
  93.3 0.9 copy-done.9
  94.2 1.1 copy-done.4
  95.3 1.1 copy-done.6
  96.5 1.1 copy-done.8
  97.6 1.1 copy-done.10
  98.7 3.2 %ffn.1 = bf16[16,256,128]{2,1,0:T(8,128)(2,1)S(1)} custom-call(bf16[16,256,128]{2,1,0:T(8,128)(2,1)} %all-to-all-done.1.tiles, bf16[2048,256]{1,0:T(8,128)(2,1)S(1)} %bitcast.12, bf16[2048,256]{1,0:T(8,128)(2,1)S(1)} %bitcast.14, bf16[256,2048]{1,0:T(8,128)(2,1)S(1)} %bitcast.16, bf16[3072,128]{1,0:T(8,128)(2,1)S(1)} %copy-done.4, ...), custom_call_target="tpu_custom_call" | custom-call | flops 1610612736 | bytes 6291456 | tf_op jit(solution)/shard_map/ffn/pallas_call | solution.py:250
  101.9 21.9 %all_to_all.21.parts = bf16[16,256,128]{2,1,0:T(8,128)(2,1)S(1)} all-to-all(bf16[16,256,128]{2,1,0:T(8,128)(2,1)S(1)} %ffn.1), channel_id=1, replica_groups=mesh['ep'=64,'tp'=16] {'tp'}, dimensions={0} | all-to-all | bytes 2097152 | tf_op jit(solution)/shard_map/all_to_all | solution.py:179
  123.9 0.8 add.1
  124.6 21.5 %all-to-all-start.3 = ((bf16[64,8,128]{2,1,0:T(8,128)(2,1)}), bf16[64,8,128]{2,1,0:T(8,128)(2,1)S(1)}, u32[]{:S(2)}, u32[]{:S(2)}) async-start(bf16[64,8,128]{2,1,0:T(8,128)(2,1)} %bitcast.8), calls=%async_computation.3 | async-start | bytes 262144 | tf_op jit(solution)/shard_map/all_to_all | solution.py:179
  146.1 0.9 place.1.places
  147.1 29.7 %all-to-all-done.3 = bf16[64,8,128]{2,1,0:T(8,128)(2,1)S(1)} async-done(((bf16[64,8,128]{2,1,0:T(8,128)(2,1)}), bf16[64,8,128]{2,1,0:T(8,128)(2,1)S(1)}, u32[]{:S(2)}, u32[]{:S(2)}) %all-to-all-start.3) | async-done | bytes 131104 | tf_op jit(solution)/shard_map/all_to_all | solution.py:179
  176.8 0.9 combine.1
  (21 shorter events, 0.8 us)
Async XLA Ops:
  50.9 8.1 %copy-start.2 = (bf16[1,256,2048]{2,1,0:T(8,128)(2,1)S(1)}, bf16[1,256,2048]{2,1,0:T(8,128)(2,1)}, u32[]{:S(2)}) copy-start(bf16[1,256,2048]{2,1,0:T(8,128)(2,1)} %param.11) | copy-start | bytes 3145732
  52.0 7.0 %copy-start = (bf16[1,2048,256]{2,1,0:T(8,128)(2,1)S(1)}, bf16[1,2048,256]{2,1,0:T(8,128)(2,1)}, u32[]{:S(2)}) copy-start(bf16[1,2048,256]{2,1,0:T(8,128)(2,1)} %param.9) | copy-start | bytes 3145732
  52.0 7.0 %copy-start.1 = (bf16[1,2048,256]{2,1,0:T(8,128)(2,1)S(1)}, bf16[1,2048,256]{2,1,0:T(8,128)(2,1)}, u32[]{:S(2)}) copy-start(bf16[1,2048,256]{2,1,0:T(8,128)(2,1)} %param.10) | copy-start | bytes 3145732
  52.0 42.2 %all-to-all-start.1 = ((bf16[16,256,128]{2,1,0:T(8,128)(2,1)}), bf16[16,256,128]{2,1,0:T(8,128)(2,1)}, u32[]{:S(2)}, u32[]{:S(2)}) async-start(bf16[16,256,128]{2,1,0:T(8,128)(2,1)} %spread.1), calls=%async_computation.1 | async-start | bytes 2097152 | tf_op jit(solution)/shard_map/all_to_all | solution.py:179
  59.7 30.9 %collective-permute-start = (bf16[3072,128]{1,0:T(8,128)(2,1)S(1)}, bf16[3072,128]{1,0:T(8,128)(2,1)S(1)}, u32[]{:S(2)}, u32[]{:S(2)}) collective-permute-start(bf16[3072,128]{1,0:T(8,128)(2,1)S(1)} %get-tuple-element.9), channel_id=1, source_target_pairs={{0,1},{1,2},{2,3},{3,0},{4,5},{5,6},{6,7},{7,4},{8,9},{9,10},{10,1... | collective-permute-start | bytes 2359304 | tf_op jit(solution)/shard_map/ppermute | solution.py:224
  63.0 28.6 %collective-permute-start.1 = (bf16[3072,128]{1,0:T(8,128)(2,1)S(1)}, bf16[3072,128]{1,0:T(8,128)(2,1)S(1)}, u32[]{:S(2)}, u32[]{:S(2)}) collective-permute-start(bf16[3072,128]{1,0:T(8,128)(2,1)S(1)} %get-tuple-element.10), channel_id=1, source_target_pairs={{0,3},{1,0},{2,1},{3,2},{4,7},{5,4},{6,5},{7,6},{8,11},{9,8},{10,9... | collective-permute-start | bytes 2359304 | tf_op jit(solution)/shard_map/ppermute | solution.py:224
  66.2 26.1 %collective-permute-start.2 = (bf16[3072,128]{1,0:T(8,128)(2,1)S(1)}, bf16[3072,128]{1,0:T(8,128)(2,1)S(1)}, u32[]{:S(2)}, u32[]{:S(2)}) collective-permute-start(bf16[3072,128]{1,0:T(8,128)(2,1)S(1)} %get-tuple-element.11), channel_id=1, source_target_pairs={{0,4},{1,5},{2,6},{3,7},{4,8},{5,9},{6,10},{7,11},{8,12},{9,13},{1... | collective-permute-start | bytes 2359304 | tf_op jit(solution)/shard_map/ppermute | solution.py:224
  69.5 23.8 %collective-permute-start.3 = (bf16[3072,128]{1,0:T(8,128)(2,1)S(1)}, bf16[3072,128]{1,0:T(8,128)(2,1)S(1)}, u32[]{:S(2)}, u32[]{:S(2)}) collective-permute-start(bf16[3072,128]{1,0:T(8,128)(2,1)S(1)} %get-tuple-element.12), channel_id=1, source_target_pairs={{0,12},{1,13},{2,14},{3,15},{4,0},{5,1},{6,2},{7,3},{8,4},{9,5},{1... | collective-permute-start | bytes 2359304 | tf_op jit(solution)/shard_map/ppermute | solution.py:224
  90.6 0.9 copy-start.3
  91.5 0.9 copy-start.5
  92.4 0.9 copy-start.7
  93.3 0.9 copy-start.9
  94.2 1.1 copy-start.4
  95.3 1.1 copy-start.6
  96.5 1.1 copy-start.8
  97.6 1.1 copy-start.10
  124.6 21.5 %copy-start.11 = (f32[1,64,8]{1,2,0:T(8,128)S(1)}, f32[1,64,8]{1,2,0:T(8,128)}, u32[]{:S(2)}) copy-start(f32[1,64,8]{1,2,0:T(8,128)} %param.8) | copy-start | bytes 6148
  124.6 52.1 %all-to-all-start.3 = ((bf16[64,8,128]{2,1,0:T(8,128)(2,1)}), bf16[64,8,128]{2,1,0:T(8,128)(2,1)S(1)}, u32[]{:S(2)}, u32[]{:S(2)}) async-start(bf16[64,8,128]{2,1,0:T(8,128)(2,1)} %bitcast.8), calls=%async_computation.3 | async-start | bytes 262144 | tf_op jit(solution)/shard_map/all_to_all | solution.py:179

commit v3 on v2

--- a/solution.py
+++ b/solution.py
@@ -10,6 +10,7 @@
 GRID = 4
 STEPS = ((0, 1), (0, -1), (1, 0), (-1, 0))
 VMEM = pl.BlockSpec(memory_space=pltpu.VMEM)
+LEAD_OUT, LEAD_BACK = 1 / 4, 1 / 2
 HBM = pl.BlockSpec(memory_space=pltpu.HBM)
 
 
@@ -37,7 +38,7 @@
     return pltpu.CompilerParams(vmem_limit_bytes=mib * 2**20)
 
 
-def pick_kernel(tokens, chosen, out, columns, picks, sems):
+def pick_kernel(first, tokens, chosen, out, columns, picks, sems):
     width = out.shape[1]
     start = pl.multiple_of(lax.axis_index("tp") * width, width)
     get_columns = pltpu.make_async_copy(tokens.at[:, pl.ds(start, width)], columns, sems.at[0])
@@ -48,7 +49,7 @@
     each, experts = picks.shape
     row = lax.broadcasted_iota(jnp.int32, (rows, experts), 0)
     expert = lax.broadcasted_iota(jnp.int32, (rows, experts), 1)
-    spread = jnp.where((row // each + experts // 2) % experts == expert, 1.0, 0.0)
+    spread = jnp.where((row // each + first) % experts == expert, 1.0, 0.0)
     spread = spread.astype(jnp.bfloat16)
     row = lax.broadcasted_iota(jnp.int32, (rows, each), 0)
     pick = lax.broadcasted_iota(jnp.int32, (rows, each), 1)
@@ -69,14 +70,15 @@
     out[...] = jnp.dot(one_hot, columns[...], preferred_element_type=jnp.float32).astype(out.dtype)
 
 
-def place_kernel(chosen, weight, out, picks, sem):
+def place_kernel(first, chosen, weight, out, picks, sem):
     get_picks = pltpu.make_async_copy(chosen.at[lax.axis_index("ep")], picks, sem)
     get_picks.start()
     each, experts = picks.shape
     tok_count, rows = out.shape[1:]
     row = lax.broadcasted_iota(jnp.int32, (experts, rows), 1)
     expert = lax.broadcasted_iota(jnp.int32, (experts, rows), 0)
-    spread = jnp.where(row // each == expert, 1.0, 0.0).astype(jnp.bfloat16)
+    spread = jnp.where((row // each + first) % experts == expert, 1.0, 0.0)
+    spread = spread.astype(jnp.bfloat16)
     row = lax.broadcasted_iota(jnp.int32, (each, rows), 1)
     pick = lax.broadcasted_iota(jnp.int32, (each, rows), 0)
     mine = row % each == pick
@@ -102,18 +104,32 @@
     out[...] = total.astype(out.dtype)
 
 
-def pack_kernel(gate, up, down, *outs):
+def pack_kernel(gate_hbm, up_hbm, down_hbm, *refs):
+    outs, (gate, up, down, packed, loads, stores) = refs[:4], refs[4:]
+    into = [
+        pltpu.make_async_copy(src, dst, loads.at[k])
+        for k, (src, dst) in enumerate(((gate_hbm, gate), (up_hbm, up), (down_hbm, down)))
+    ]
+    for copy in into:
+        copy.start()
     depth, units = gate.shape
     part = units // len(outs)
     lanes = 2 * part
+    for copy in into:
+        copy.wait()
+    leave = []
     for q, out in enumerate(outs):
         g = gate[:, q * part : (q + 1) * part]
         u = up[:, q * part : (q + 1) * part]
-        out[:depth, :] = jnp.concatenate([g, u] if q % 2 == 0 else [u, g], axis=1)
+        packed[q, :depth, :] = jnp.concatenate([g, u] if q % 2 == 0 else [u, g], axis=1)
         for c in range(down.shape[1] // lanes):
-            out[depth + c * part : depth + (c + 1) * part, :] = down[
+            packed[q, depth + c * part : depth + (c + 1) * part, :] = down[
                 q * part : (q + 1) * part, c * lanes : (c + 1) * lanes
             ]
+        leave.append(pltpu.make_async_copy(packed.at[q], out, stores.at[q]))
+        leave[-1].start()
+    for copy in leave:
+        copy.wait()
 
 
 def spread_kernel(rows, out):
@@ -162,15 +178,17 @@
         out[c + 1] = sums[:, lanes:]
 
 
-def sum_kernel(parts, out):
-    half = parts.shape[1]
+def sum_kernel(shift, parts, out):
+    half, rows = parts.shape[1], out.shape[0]
     for k in range(2):
         total = None
         for u in range(parts.shape[0]):
             if colour(u) == k:
                 term = parts[u].astype(jnp.float32)
                 total = term if total is None else total + term
-        out[(1 - k) * half : (2 - k) * half, :] = total.astype(out.dtype)
+        for r in range(0, half, shift):
+            to = (k * half + r - shift) % rows
+            out[to : to + shift, :] = total[r : r + shift, :].astype(out.dtype)
 
 
 def exchange(tiles, axis, first=0):
@@ -187,13 +205,14 @@
     blocks, experts, picks_each = chosen.shape
     width = model_width // tp_count
     count = blocks * picks_each
+    out_first, back_first = int(LEAD_OUT * experts), int(LEAD_BACK * experts)
     gate, up, down = gate_weight[0], up_weight[0], down_weight[0]
     units = gate.shape[1]
     bf16 = functools.partial(jax.ShapeDtypeStruct, dtype=jnp.bfloat16)
 
     by_pick = in_hbm(jnp.transpose(chosen, (0, 2, 1)))
     leaving = pl.pallas_call(
-        pick_kernel,
+        functools.partial(pick_kernel, out_first),
         out_shape=bf16((count, width)),
         in_specs=[HBM, HBM],
         out_specs=VMEM,
@@ -207,26 +226,34 @@
         name="pick",
     )(in_hbm(tokens), by_pick)
     arrived = exchange(
-        leaving.reshape(experts, picks_each, width), "ep", experts // 2
+        leaving.reshape(experts, picks_each, width), "ep", out_first
     ).reshape(count, width)
 
     pack = pl.pallas_call(
         pack_kernel,
         out_shape=[bf16((model_width + model_width // 2, units // 2))] * 4,
-        in_specs=[VMEM] * 3,
-        out_specs=[VMEM] * 4,
+        in_specs=[HBM] * 3,
+        out_specs=[HBM] * 4,
+        scratch_shapes=[
+            pltpu.VMEM(gate.shape, jnp.bfloat16),
+            pltpu.VMEM(up.shape, jnp.bfloat16),
+            pltpu.VMEM(down.shape, jnp.bfloat16),
+            pltpu.VMEM((4, model_width + model_width // 2, units // 2), jnp.bfloat16),
+            pltpu.SemaphoreType.DMA((3,)),
+            pltpu.SemaphoreType.DMA((4,)),
+        ],
         compiler_params=room(12),
         cost_estimate=cost(10**8, 12 * model_width * units),
         name="pack",
     )
-    packs = pack(gate, up, down)
+    packs = pack(in_hbm(gate), in_hbm(up), in_hbm(down))
     shared = [
         lax.ppermute(pack, "tp", neighbour_pairs(*step))
         for pack, step in zip(packs, STEPS, strict=True)
     ]
 
     place = pl.pallas_call(
-        place_kernel,
+        functools.partial(place_kernel, back_first),
         out_shape=bf16((3, tok_count, count)),
         in_specs=[HBM, VMEM],
         out_specs=VMEM,
@@ -259,7 +286,7 @@
     )(tiles, gate, up, down, *shared)
     partial = exchange(partial, "tp")
     expert_out = pl.pallas_call(
-        sum_kernel,
+        functools.partial(sum_kernel, (back_first - out_first) * picks_each),
         out_shape=bf16((count, width)),
         in_specs=[VMEM],
         out_specs=VMEM,
@@ -267,9 +294,9 @@
         cost_estimate=cost(10**8, tp_count * count * width),
         name="add",
     )(partial)
-    returned = exchange(expert_out.reshape(blocks, picks_each, width), "ep").reshape(
-        experts * picks_each, width
-    )
+    returned = exchange(
+        expert_out.reshape(blocks, picks_each, width), "ep", back_first
+    ).reshape(experts * picks_each, width)
     return pl.pallas_call(
         combine_kernel,
         out_shape=bf16((tok_count, width)),

time: 178 us -> 170 us (0.955)
  waiting for transfers between devices: 47.6 us -> 26.8 us
  blocking collectives: 71.6 us -> 77.9 us
  starting transfers between devices: 41.4 us -> 44.7 us
  Pallas kernels: 8.87 us -> 11.3 us
    all_to_all x2, waiting for transfers between devices: 29.7 us -> 11.4 us  [exchange(): lax.all_to_all(tiles, axis, split_axis=0, concat_axis=0, axis_index_group...]
    all_to_all x2, blocking collectives: 71.6 us -> 77.9 us  [exchange(): lax.all_to_all(tiles, axis, split_axis=0, concat_axis=0, axis_index_group...]
    all_to_all x2, starting transfers between devices: 28.4 us -> 31.7 us  [exchange(): lax.all_to_all(tiles, axis, split_axis=0, concat_axis=0, axis_index_group...]
    ppermute x4, waiting for transfers between devices: 17.9 us -> 15.4 us  [local(): lax.ppermute(pack, 'tp', neighbour_pairs(*step))]
    pallas_call x3, Pallas kernels: 2.77 us -> 5.24 us  [the longest x1 3.22 us: local(): packs = pack(in_hbm(gate), in_hbm(up), in_hbm(down))]
  transfers between devices with their start and end apart: 6 -> 6, of which waited for: 2 -> 2; matrix products, arithmetic and copies ran while one was open for 0% -> 0% of each run, Pallas kernels for 1% -> 2%
where the time goes in v3:
time: 170 us; the launch traced here: 169 us
  blocking collectives  77.9 us (46%)
  starting transfers between devices  44.7 us (26%)
  waiting for transfers between devices  26.8 us (16%)
  Pallas kernels  11.3 us (7%)
  local copies, waits for them, and re-layouts  8.1 us (5%)
    all_to_all x2, blocking collectives, exchange(): lax.all_to_all(tiles, axis, split_axis=0, concat_axis=0, axis_index_group...  77.9 us
    all_to_all x2, starting transfers between devices, exchange(): lax.all_to_all(tiles, axis, split_axis=0, concat_axis=0, axis_index_group...  31.7 us
    ppermute x4, waiting for transfers between devices, local(): lax.ppermute(pack, 'tp', neighbour_pairs(*step))  15.4 us
    ppermute x4, starting transfers between devices, local(): lax.ppermute(pack, 'tp', neighbour_pairs(*step))  13 us
    all_to_all x2, waiting for transfers between devices, exchange(): lax.all_to_all(tiles, axis, split_axis=0, concat_axis=0, axis_index_group...  11.4 us
    unnamed x24, local copies, waits for them, and re-layouts  8.1 us
  transfers between devices with their start and end apart: 6, of which 2 were waited for; matrix products, arithmetic and copies ran while one was open for 0% of the time, Pallas kernels for 2%

profile of v3, /device:TPU:1, one launch (start us, length us, event | category | flops | bytes accessed | tf_op | source)
XLA Modules:
  0.0 169.0 jit_solution(12706806376855921895)
XLA Ops:
  0.0 1.2 pick.1
  1.2 56.0 %all_to_all.20 = bf16[64,8,128]{2,1,0:T(8,128)(2,1)S(1)} all-to-all(bf16[64,8,128]{2,1,0:T(8,128)(2,1)S(1)} %bitcast.19), channel_id=1, replica_groups={{256,272,288,304,320,336,352,368,384,400,416,432,448,464,480,496,512,52..., dimensions={0} | all-to-all | bytes 262144 | tf_op jit(solution)/shard_map/all_to_all | solution.py:197
  57.2 1.1 spread.1
  58.3 6.8 %all-to-all-start.1 = ((bf16[16,256,128]{2,1,0:T(8,128)(2,1)}), bf16[16,256,128]{2,1,0:T(8,128)(2,1)}, u32[]{:S(2)}, u32[]{:S(2)}) async-start(bf16[16,256,128]{2,1,0:T(8,128)(2,1)} %spread.1), calls=%async_computation.1 | async-start | bytes 2097152 | tf_op jit(solution)/shard_map/all_to_all | solution.py:197
  65.2 3.2 %pack.1 = (bf16[3072,128]{1,0:T(8,128)(2,1)S(1)}, bf16[3072,128]{1,0:T(8,128)(2,1)S(1)}, bf16[3072,128]{1,0:T(8,128)(2,1)S(1)}, bf16[3072,128]{1,0:T(8,128)(2,1)S(1)}) custom-call(bf16[2048,256]{1,0:T(8,128)(2,1)} %bitcast.11, bf16[2048,256]{1,0:T(8,128)(2,1)} %bitcast.13, bf16[256,2048]{1,0:T(8,128)(2,1)} %bitcast.15), custom_call_target="tpu_custom_call" | custom-call | flops 100000000 | bytes 6291456 | tf_op jit(solution)/shard_map/pack/pallas_call | solution.py:249
  68.4 3.2 %collective-permute-start = (bf16[3072,128]{1,0:T(8,128)(2,1)S(1)}, bf16[3072,128]{1,0:T(8,128)(2,1)S(1)}, u32[]{:S(2)}, u32[]{:S(2)}) collective-permute-start(bf16[3072,128]{1,0:T(8,128)(2,1)S(1)} %get-tuple-element.9), channel_id=1, source_target_pairs={{0,1},{1,2},{2,3},{3,0},{4,5},{5,6},{6,7},{7,4},{8,9},{9,10},{10,1... | collective-permute-start | bytes 2359304 | tf_op jit(solution)/shard_map/ppermute | solution.py:251
  71.7 3.3 %collective-permute-start.1 = (bf16[3072,128]{1,0:T(8,128)(2,1)S(1)}, bf16[3072,128]{1,0:T(8,128)(2,1)S(1)}, u32[]{:S(2)}, u32[]{:S(2)}) collective-permute-start(bf16[3072,128]{1,0:T(8,128)(2,1)S(1)} %get-tuple-element.10), channel_id=1, source_target_pairs={{0,3},{1,0},{2,1},{3,2},{4,7},{5,4},{6,5},{7,6},{8,11},{9,8},{10,9... | collective-permute-start | bytes 2359304 | tf_op jit(solution)/shard_map/ppermute | solution.py:251
  75.0 3.2 %collective-permute-start.2 = (bf16[3072,128]{1,0:T(8,128)(2,1)S(1)}, bf16[3072,128]{1,0:T(8,128)(2,1)S(1)}, u32[]{:S(2)}, u32[]{:S(2)}) collective-permute-start(bf16[3072,128]{1,0:T(8,128)(2,1)S(1)} %get-tuple-element.11), channel_id=1, source_target_pairs={{0,4},{1,5},{2,6},{3,7},{4,8},{5,9},{6,10},{7,11},{8,12},{9,13},{1... | collective-permute-start | bytes 2359304 | tf_op jit(solution)/shard_map/ppermute | solution.py:251
  78.2 3.3 %collective-permute-start.3 = (bf16[3072,128]{1,0:T(8,128)(2,1)S(1)}, bf16[3072,128]{1,0:T(8,128)(2,1)S(1)}, u32[]{:S(2)}, u32[]{:S(2)}) collective-permute-start(bf16[3072,128]{1,0:T(8,128)(2,1)S(1)} %get-tuple-element.12), channel_id=1, source_target_pairs={{0,12},{1,13},{2,14},{3,15},{4,0},{5,1},{6,2},{7,3},{8,4},{9,5},{1... | collective-permute-start | bytes 2359304 | tf_op jit(solution)/shard_map/ppermute | solution.py:251
  81.5 15.4 %collective-permute-done.p0 = bf16[3072,128]{1,0:T(8,128)(2,1)S(1)} collective-permute-done((bf16[3072,128]{1,0:T(8,128)(2,1)S(1)}, bf16[3072,128]{1,0:T(8,128)(2,1)S(1)}, u32[]{:S(2)}, u32[]{:S(2)}) %collective-permute-start) | collective-permute-done | bytes 786464 | tf_op jit(solution)/shard_map/ppermute | solution.py:251
  96.9 0.9 copy-done.3
  97.7 0.9 copy-done.5
  98.6 0.9 copy-done.7
  99.5 0.9 copy-done.9
  100.5 1.1 copy-done.4
  101.6 1.1 copy-done.6
  102.7 1.1 copy-done.8
  103.9 1.1 copy-done.10
  105.0 3.2 %ffn.1 = bf16[16,256,128]{2,1,0:T(8,128)(2,1)S(1)} custom-call(bf16[16,256,128]{2,1,0:T(8,128)(2,1)} %all-to-all-done.1.tiles, bf16[2048,256]{1,0:T(8,128)(2,1)S(1)} %bitcast.12, bf16[2048,256]{1,0:T(8,128)(2,1)S(1)} %bitcast.14, bf16[256,2048]{1,0:T(8,128)(2,1)S(1)} %bitcast.16, bf16[3072,128]{1,0:T(8,128)(2,1)S(1)} %copy-done.4, ...), custom_call_target="tpu_custom_call" | custom-call | flops 1610612736 | bytes 6291456 | tf_op jit(solution)/shard_map/ffn/pallas_call | solution.py:277
  108.2 21.9 %all_to_all.21.parts = bf16[16,256,128]{2,1,0:T(8,128)(2,1)S(1)} all-to-all(bf16[16,256,128]{2,1,0:T(8,128)(2,1)S(1)} %ffn.1), channel_id=1, replica_groups=mesh['ep'=64,'tp'=16] {'tp'}, dimensions={0} | all-to-all | bytes 2097152 | tf_op jit(solution)/shard_map/all_to_all | solution.py:197
  130.9 24.8 %all-to-all-start.3 = ((bf16[64,8,128]{2,1,0:T(8,128)(2,1)}), bf16[64,8,128]{2,1,0:T(8,128)(2,1)S(1)}, u32[]{:S(2)}, u32[]{:S(2)}) async-start(bf16[64,8,128]{2,1,0:T(8,128)(2,1)} %bitcast.8), calls=%async_computation.3 | async-start | bytes 262144 | tf_op jit(solution)/shard_map/all_to_all | solution.py:197
  155.7 0.9 place.1.places
  156.7 11.4 %all-to-all-done.3 = bf16[64,8,128]{2,1,0:T(8,128)(2,1)S(1)} async-done(((bf16[64,8,128]{2,1,0:T(8,128)(2,1)}), bf16[64,8,128]{2,1,0:T(8,128)(2,1)S(1)}, u32[]{:S(2)}, u32[]{:S(2)}) %all-to-all-start.3) | async-done | bytes 131104 | tf_op jit(solution)/shard_map/all_to_all | solution.py:197
  168.1 0.9 combine.1
  (21 shorter events, 0.8 us)
Async XLA Ops:
  58.3 42.1 %all-to-all-start.1 = ((bf16[16,256,128]{2,1,0:T(8,128)(2,1)}), bf16[16,256,128]{2,1,0:T(8,128)(2,1)}, u32[]{:S(2)}, u32[]{:S(2)}) async-start(bf16[16,256,128]{2,1,0:T(8,128)(2,1)} %spread.1), calls=%async_computation.1 | async-start | bytes 2097152 | tf_op jit(solution)/shard_map/all_to_all | solution.py:197
  65.2 35.3 %copy-start = (bf16[1,2048,256]{2,1,0:T(8,128)(2,1)S(1)}, bf16[1,2048,256]{2,1,0:T(8,128)(2,1)}, u32[]{:S(2)}) copy-start(bf16[1,2048,256]{2,1,0:T(8,128)(2,1)} %param.9) | copy-start | bytes 3145732
  65.2 35.2 %copy-start.1 = (bf16[1,2048,256]{2,1,0:T(8,128)(2,1)S(1)}, bf16[1,2048,256]{2,1,0:T(8,128)(2,1)}, u32[]{:S(2)}) copy-start(bf16[1,2048,256]{2,1,0:T(8,128)(2,1)} %param.10) | copy-start | bytes 3145732
  65.2 35.2 %copy-start.2 = (bf16[1,256,2048]{2,1,0:T(8,128)(2,1)S(1)}, bf16[1,256,2048]{2,1,0:T(8,128)(2,1)}, u32[]{:S(2)}) copy-start(bf16[1,256,2048]{2,1,0:T(8,128)(2,1)} %param.11) | copy-start | bytes 3145732
  68.4 28.4 %collective-permute-start = (bf16[3072,128]{1,0:T(8,128)(2,1)S(1)}, bf16[3072,128]{1,0:T(8,128)(2,1)S(1)}, u32[]{:S(2)}, u32[]{:S(2)}) collective-permute-start(bf16[3072,128]{1,0:T(8,128)(2,1)S(1)} %get-tuple-element.9), channel_id=1, source_target_pairs={{0,1},{1,2},{2,3},{3,0},{4,5},{5,6},{6,7},{7,4},{8,9},{9,10},{10,1... | collective-permute-start | bytes 2359304 | tf_op jit(solution)/shard_map/ppermute | solution.py:251
  71.7 26.1 %collective-permute-start.1 = (bf16[3072,128]{1,0:T(8,128)(2,1)S(1)}, bf16[3072,128]{1,0:T(8,128)(2,1)S(1)}, u32[]{:S(2)}, u32[]{:S(2)}) collective-permute-start(bf16[3072,128]{1,0:T(8,128)(2,1)S(1)} %get-tuple-element.10), channel_id=1, source_target_pairs={{0,3},{1,0},{2,1},{3,2},{4,7},{5,4},{6,5},{7,6},{8,11},{9,8},{10,9... | collective-permute-start | bytes 2359304 | tf_op jit(solution)/shard_map/ppermute | solution.py:251
  75.0 23.7 %collective-permute-start.2 = (bf16[3072,128]{1,0:T(8,128)(2,1)S(1)}, bf16[3072,128]{1,0:T(8,128)(2,1)S(1)}, u32[]{:S(2)}, u32[]{:S(2)}) collective-permute-start(bf16[3072,128]{1,0:T(8,128)(2,1)S(1)} %get-tuple-element.11), channel_id=1, source_target_pairs={{0,4},{1,5},{2,6},{3,7},{4,8},{5,9},{6,10},{7,11},{8,12},{9,13},{1... | collective-permute-start | bytes 2359304 | tf_op jit(solution)/shard_map/ppermute | solution.py:251
  78.2 21.3 %collective-permute-start.3 = (bf16[3072,128]{1,0:T(8,128)(2,1)S(1)}, bf16[3072,128]{1,0:T(8,128)(2,1)S(1)}, u32[]{:S(2)}, u32[]{:S(2)}) collective-permute-start(bf16[3072,128]{1,0:T(8,128)(2,1)S(1)} %get-tuple-element.12), channel_id=1, source_target_pairs={{0,12},{1,13},{2,14},{3,15},{4,0},{5,1},{6,2},{7,3},{8,4},{9,5},{1... | collective-permute-start | bytes 2359304 | tf_op jit(solution)/shard_map/ppermute | solution.py:251
  96.9 0.9 copy-start.3
  97.7 0.9 copy-start.5
  98.6 0.9 copy-start.7
  99.5 0.9 copy-start.9
  100.4 1.1 copy-start.4
  101.6 1.1 copy-start.6
  102.7 1.1 copy-start.8
  103.8 1.1 copy-start.10
  130.9 24.9 %copy-start.11 = (f32[1,64,8]{1,2,0:T(8,128)S(1)}, f32[1,64,8]{1,2,0:T(8,128)}, u32[]{:S(2)}) copy-start(f32[1,64,8]{1,2,0:T(8,128)} %param.8) | copy-start | bytes 6148
  130.9 37.2 %all-to-all-start.3 = ((bf16[64,8,128]{2,1,0:T(8,128)(2,1)}), bf16[64,8,128]{2,1,0:T(8,128)(2,1)S(1)}, u32[]{:S(2)}, u32[]{:S(2)}) async-start(bf16[64,8,128]{2,1,0:T(8,128)(2,1)} %bitcast.8), calls=%async_computation.3 | async-start | bytes 262144 | tf_op jit(solution)/shard_map/all_to_all | solution.py:197

commit v4 on v3

--- a/solution.py
+++ b/solution.py
@@ -8,9 +8,10 @@
 from jax.sharding import PartitionSpec as P
 
 GRID = 4
-STEPS = ((0, 1), (0, -1), (1, 0), (-1, 0))
+STEPS = (((0, 1), (0, -1)), ((1, 0), (-1, 0)))
 VMEM = pl.BlockSpec(memory_space=pltpu.VMEM)
-LEAD_OUT, LEAD_BACK = 1 / 4, 1 / 2
+LEAD_OUT, LEAD_BACK = 1 / 2, 1 / 2
+ANY = pl.BlockSpec(memory_space=pl.ANY)
 HBM = pl.BlockSpec(memory_space=pltpu.HBM)
 
 
@@ -18,12 +19,15 @@
     return (u // GRID + u % GRID) % 2
 
 
-def neighbour_pairs(dy, dx):
-    return [
-        (y * GRID + x, (y + dy) % GRID * GRID + (x + dx) % GRID)
-        for y in range(GRID)
-        for x in range(GRID)
-    ]
+def neighbour_pairs(which, ep_count):
+    pairs = []
+    for e in range(ep_count):
+        dy, dx = STEPS[e % 2][which]
+        for y in range(GRID):
+            for x in range(GRID):
+                to = (y + dy) % GRID * GRID + (x + dx) % GRID
+                pairs.append((e * GRID**2 + y * GRID + x, e * GRID**2 + to))
+    return pairs
 
 
 def cost(flops, nbytes):
@@ -104,78 +108,89 @@
     out[...] = total.astype(out.dtype)
 
 
-def pack_kernel(gate_hbm, up_hbm, down_hbm, *refs):
-    outs, (gate, up, down, packed, loads, stores) = refs[:4], refs[4:]
-    into = [
-        pltpu.make_async_copy(src, dst, loads.at[k])
-        for k, (src, dst) in enumerate(((gate_hbm, gate), (up_hbm, up), (down_hbm, down)))
-    ]
-    for copy in into:
-        copy.start()
+def pack_kernel(gate, up, down, *refs):
+    outs, (packed, loads, stores) = refs[:2], refs[2:]
     depth, units = gate.shape
-    part = units // len(outs)
-    lanes = 2 * part
-    for copy in into:
-        copy.wait()
+    part = units // 2
+    into = []
+    for q in range(2):
+        mine = pl.ds(q * part, part)
+        target = packed.at[q]
+        top = pl.ds(0, depth)
+        copies = [
+            (gate.at[:, mine], target.at[top, pl.ds(0, part)]),
+            (up.at[:, mine], target.at[top, pl.ds(part, part)]),
+        ]
+        for c in range(depth // units):
+            copies.append(
+                (
+                    down.at[mine, pl.ds(c * units, units)],
+                    target.at[pl.ds(depth + c * part, part), :],
+                )
+            )
+        into.append([pltpu.make_async_copy(*ends, loads.at[q, k]) for k, ends in enumerate(copies)])
+    for copies in into:
+        for copy in copies:
+            copy.start()
     leave = []
     for q, out in enumerate(outs):
-        g = gate[:, q * part : (q + 1) * part]
-        u = up[:, q * part : (q + 1) * part]
-        packed[q, :depth, :] = jnp.concatenate([g, u] if q % 2 == 0 else [u, g], axis=1)
-        for c in range(down.shape[1] // lanes):
-            packed[q, depth + c * part : depth + (c + 1) * part, :] = down[
-                q * part : (q + 1) * part, c * lanes : (c + 1) * lanes
-            ]
+        for copy in into[q]:
+            copy.wait()
         leave.append(pltpu.make_async_copy(packed.at[q], out, stores.at[q]))
         leave[-1].start()
     for copy in leave:
         copy.wait()
 
 
-def spread_kernel(rows, out):
+def spread_kernel(rows, out, stores):
     half = out.shape[1]
-    for u in range(out.shape[0]):
-        out[u] = rows[colour(u) * half : (colour(u) + 1) * half, :]
+    copies = [
+        pltpu.make_async_copy(rows.at[pl.ds(colour(u) * half, half), :], out.at[u], stores.at[u])
+        for u in range(out.shape[0])
+    ]
+    for copy in copies:
+        copy.start()
+    for copy in copies:
+        copy.wait()
 
 
 def silu(v):
     return v / (1.0 + jnp.exp(-v))
 
 
-def ffn_kernel(tiles, gate, up, down, p0, p1, p2, p3, out, rows):
-    chunks, count, lanes = tiles.shape
+def ffn_kernel(tiles, gate, up, d_hbm, p0_hbm, p1_hbm, out, rows, p0, p1, down, row_sems, p_sems):
+    chunks, _, lanes = tiles.shape
     depth, units = gate.shape
-    part = units // 4
-    for t in range(chunks):
-        rows[:, t * lanes : (t + 1) * lanes] = tiles[t]
-    low = lax.broadcasted_iota(jnp.int32, (count, lanes), 1) < part
+    part = units // 2
+    get_rows = [
+        pltpu.make_async_copy(tiles.at[t], rows.at[:, pl.ds(t * lanes, lanes)], row_sems.at[t])
+        for t in range(chunks)
+    ]
+    get_shared = [
+        pltpu.make_async_copy(src, dst, p_sems.at[k])
+        for k, (src, dst) in enumerate(((p0_hbm, p0), (p1_hbm, p1), (d_hbm, down)))
+    ]
+    for copy in get_rows + get_shared:
+        copy.start()
+    for copy in get_rows:
+        copy.wait()
     gate_sum = jnp.dot(rows[...], gate[...], preferred_element_type=jnp.float32)
     up_sum = jnp.dot(rows[...], up[...], preferred_element_type=jnp.float32)
     hidden = [(silu(gate_sum) * up_sum).astype(jnp.bfloat16)]
-    for a, b in ((p0, p1), (p2, p3)):
-        both = jnp.dot(
-            rows[...],
-            jnp.concatenate([a[:depth, :], b[:depth, :]], axis=1),
-            preferred_element_type=jnp.float32,
-        )
-        left, right = both[:, :lanes], both[:, lanes:]
-        left = silu(left) * pltpu.roll(left, part, 1)
-        right = silu(right) * pltpu.roll(right, part, 1)
-        hidden.append(jnp.where(low, left, right).astype(jnp.bfloat16))
+    for p, copy in zip((p0, p1), get_shared[:2], strict=True):
+        copy.wait()
+        both = jnp.dot(rows[...], p[:depth, :], preferred_element_type=jnp.float32)
+        hidden.append((silu(both[:, :part]) * both[:, part:]).astype(jnp.bfloat16))
     hidden = jnp.concatenate(hidden, axis=1)
-    for c in range(0, chunks, 2):
-        theirs = [
-            jnp.concatenate(
-                [p[depth + k * part : depth + (k + 1) * part, :] for p in (p0, p1, p2, p3)], axis=0
-            )
-            for k in (c, c + 1)
-        ]
+    get_shared[2].wait()
+    for c in range(depth // units):
+        theirs = pl.ds(depth + c * part, part)
         weights = jnp.concatenate(
-            [down[:, c * lanes : (c + 2) * lanes], jnp.concatenate(theirs, axis=1)], axis=0
+            [down[:, c * units : (c + 1) * units], p0[theirs, :], p1[theirs, :]], axis=0
         )
         sums = jnp.dot(hidden, weights, preferred_element_type=jnp.float32).astype(out.dtype)
-        out[c] = sums[:, :lanes]
-        out[c + 1] = sums[:, lanes:]
+        for k in range(units // lanes):
+            out[c * (units // lanes) + k] = sums[:, k * lanes : (k + 1) * lanes]
 
 
 def sum_kernel(shift, parts, out):
@@ -186,9 +201,10 @@
             if colour(u) == k:
                 term = parts[u].astype(jnp.float32)
                 total = term if total is None else total + term
-        for r in range(0, half, shift):
+        step = shift or half
+        for r in range(0, half, step):
             to = (k * half + r - shift) % rows
-            out[to : to + shift, :] = total[r : r + shift, :].astype(out.dtype)
+            out[to : to + step, :] = total[r : r + step, :].astype(out.dtype)
 
 
 def exchange(tiles, axis, first=0):
@@ -229,27 +245,25 @@
         leaving.reshape(experts, picks_each, width), "ep", out_first
     ).reshape(count, width)
 
+    packed = (model_width + model_width // 2, units)
     pack = pl.pallas_call(
         pack_kernel,
-        out_shape=[bf16((model_width + model_width // 2, units // 2))] * 4,
+        out_shape=[bf16(packed)] * 2,
         in_specs=[HBM] * 3,
-        out_specs=[HBM] * 4,
+        out_specs=[HBM] * 2,
         scratch_shapes=[
-            pltpu.VMEM(gate.shape, jnp.bfloat16),
-            pltpu.VMEM(up.shape, jnp.bfloat16),
-            pltpu.VMEM(down.shape, jnp.bfloat16),
-            pltpu.VMEM((4, model_width + model_width // 2, units // 2), jnp.bfloat16),
-            pltpu.SemaphoreType.DMA((3,)),
-            pltpu.SemaphoreType.DMA((4,)),
+            pltpu.VMEM((2, *packed), jnp.bfloat16),
+            pltpu.SemaphoreType.DMA((2, 2 + model_width // units)),
+            pltpu.SemaphoreType.DMA((2,)),
         ],
-        compiler_params=room(12),
+        compiler_params=room(6),
         cost_estimate=cost(10**8, 12 * model_width * units),
         name="pack",
     )
     packs = pack(in_hbm(gate), in_hbm(up), in_hbm(down))
     shared = [
-        lax.ppermute(pack, "tp", neighbour_pairs(*step))
-        for pack, step in zip(packs, STEPS, strict=True)
+        lax.ppermute(pack, ("ep", "tp"), neighbour_pairs(which, experts))
+        for which, pack in enumerate(packs)
     ]
 
     place = pl.pallas_call(
@@ -268,8 +282,9 @@
         spread_kernel,
         out_shape=bf16((tp_count, count // 2, width)),
         in_specs=[VMEM],
-        out_specs=VMEM,
-        compiler_params=room(6),
+        out_specs=HBM,
+        scratch_shapes=[pltpu.SemaphoreType.DMA((tp_count,))],
+        compiler_params=room(2),
         cost_estimate=cost(10**8, tp_count * count * width),
         name="spread",
     )(arrived)
@@ -277,13 +292,20 @@
     partial = pl.pallas_call(
         ffn_kernel,
         out_shape=bf16((tp_count, count // 2, width)),
-        in_specs=[VMEM] * 8,
-        out_specs=VMEM,
-        scratch_shapes=[pltpu.VMEM((count // 2, model_width), jnp.bfloat16)],
+        in_specs=[ANY, VMEM, VMEM, HBM, HBM, HBM],
+        out_specs=VMEM,
+        scratch_shapes=[
+            pltpu.VMEM((count // 2, model_width), jnp.bfloat16),
+            pltpu.VMEM(packed, jnp.bfloat16),
+            pltpu.VMEM(packed, jnp.bfloat16),
+            pltpu.VMEM(down.shape, jnp.bfloat16),
+            pltpu.SemaphoreType.DMA((tp_count,)),
+            pltpu.SemaphoreType.DMA((3,)),
+        ],
         cost_estimate=cost(6 * count * model_width * units, 12 * model_width * units),
         compiler_params=room(20),
         name="ffn",
-    )(tiles, gate, up, down, *shared)
+    )(tiles, gate, up, in_hbm(down), *map(in_hbm, shared))
     partial = exchange(partial, "tp")
     expert_out = pl.pallas_call(
         functools.partial(sum_kernel, (back_first - out_first) * picks_each),

time: 170 us -> 143 us (0.84)
  blocking collectives: 77.9 us -> 21.5 us
  starting transfers between devices: 44.7 us -> 76.8 us
  local copies, waits for them, and re-layouts: 8.1 us -> 0.01 us
  waiting for transfers between devices: 26.8 us -> 31.7 us
    all_to_all x2 -> x1, blocking collectives: 77.9 us -> 21.5 us  [exchange(): lax.all_to_all(tiles, axis, split_axis=0, concat_axis=0, axis_index_group...]
    all_to_all x2 -> x3, starting transfers between devices: 31.7 us -> 70.2 us  [exchange(): lax.all_to_all(tiles, axis, split_axis=0, concat_axis=0, axis_index_group...]
    unnamed x24 -> x6, local copies, waits for them, and re-layouts: 8.1 us -> 0.01 us
    ppermute x4 -> x2, starting transfers between devices: 13 us -> 6.57 us  [local(): lax.ppermute(pack, ('ep', 'tp'), neighbour_pairs(which, experts))]
    all_to_all x2 -> x3, waiting for transfers between devices: 11.4 us -> 15.4 us  [exchange(): lax.all_to_all(tiles, axis, split_axis=0, concat_axis=0, axis_index_group...]
    ppermute x4 -> x2, waiting for transfers between devices: 15.4 us -> 16.3 us  [local(): lax.ppermute(pack, ('ep', 'tp'), neighbour_pairs(which, experts))]
  transfers between devices with their start and end apart: 6 -> 5, of which waited for: 2 -> 5; matrix products, arithmetic and copies ran while one was open for 0% -> 0% of each run, Pallas kernels for 2% -> 4%
where the time goes in v4:
time: 143 us
  starting transfers between devices  76.8 us (54%)
  waiting for transfers between devices  31.7 us (22%)
  blocking collectives  21.5 us (15%)
  Pallas kernels  12.8 us (9%)
    all_to_all x3, starting transfers between devices, exchange(): lax.all_to_all(tiles, axis, split_axis=0, concat_axis=0, axis_index_group...  70.2 us
    all_to_all x1, blocking collectives, exchange(): lax.all_to_all(tiles, axis, split_axis=0, concat_axis=0, axis_index_group...  21.5 us
    ppermute x2, waiting for transfers between devices, local(): lax.ppermute(pack, ('ep', 'tp'), neighbour_pairs(which, experts))  16.3 us
    all_to_all x3, waiting for transfers between devices, exchange(): lax.all_to_all(tiles, axis, split_axis=0, concat_axis=0, axis_index_group...  15.4 us
    ppermute x2, starting transfers between devices, local(): lax.ppermute(pack, ('ep', 'tp'), neighbour_pairs(which, experts))  6.57 us
    pallas_call x1, Pallas kernels, local(): pl.pallas_call(ffn_kernel, out_shape=bf16((tp_count, count // 2, width)),...  4 us
    pallas_call x1, Pallas kernels, local(): packs = pack(in_hbm(gate), in_hbm(up), in_hbm(down))  3.17 us
  transfers between devices with their start and end apart: 5, of which 5 were waited for; matrix products, arithmetic and copies ran while one was open for 0% of the time, Pallas kernels for 4%

profile of v4, /device:TPU:1, one launch (start us, length us, event | category | flops | bytes accessed | tf_op | source)
XLA Modules:
  0.0 142.8 jit_solution(16174969737558030676)
XLA Ops:
  0.0 1.9 %pick.1 = bf16[512,128]{1,0:T(8,128)(2,1)} custom-call(bf16[128,2048]{1,0:T(8,128)(2,1)} %tokens.1, s32[64,8,64]{2,1,0:T(8,128)} %bitcast.20), custom_call_target="tpu_custom_call" | custom-call | flops 16777216 | bytes 262144 | tf_op jit(solution)/shard_map/pick/pallas_call | solution.py:230
  1.9 37.5 %all-to-all-start = ((bf16[64,8,128]{2,1,0:T(8,128)(2,1)}), bf16[64,8,128]{2,1,0:T(8,128)(2,1)S(1)}, u32[]{:S(2)}, u32[]{:S(2)}) async-start(bf16[64,8,128]{2,1,0:T(8,128)(2,1)} %bitcast.3), calls=%async_computation | async-start | bytes 262144 | tf_op jit(solution)/shard_map/all_to_all | solution.py:213
  39.4 3.2 %pack.1 = (bf16[3072,256]{1,0:T(8,128)(2,1)}, bf16[3072,256]{1,0:T(8,128)(2,1)}) custom-call(bf16[2048,256]{1,0:T(8,128)(2,1)} %bitcast.11, bf16[2048,256]{1,0:T(8,128)(2,1)} %bitcast.13, bf16[256,2048]{1,0:T(8,128)(2,1)} %bitcast.18), custom_call_target="tpu_custom_call" | custom-call | flops 100000000 | bytes 6291456 | tf_op jit(solution)/shard_map/pack/pallas_call | solution.py:263
  42.6 3.2 %collective-permute-start = (bf16[3072,256]{1,0:T(8,128)(2,1)}, bf16[3072,256]{1,0:T(8,128)(2,1)}, u32[]{:S(2)}, u32[]{:S(2)}) collective-permute-start(bf16[3072,256]{1,0:T(8,128)(2,1)} %get-tuple-element.7), channel_id=1, source_target_pairs={{0,1},{1,2},{2,3},{3,0},{4,5},{5,6},{6,7},{7,4},{8,9},{9,10},{10,1... | collective-permute-start | bytes 4718600 | tf_op jit(solution)/shard_map/ppermute | solution.py:265
  45.8 3.4 %collective-permute-start.1 = (bf16[3072,256]{1,0:T(8,128)(2,1)}, bf16[3072,256]{1,0:T(8,128)(2,1)}, u32[]{:S(2)}, u32[]{:S(2)}) collective-permute-start(bf16[3072,256]{1,0:T(8,128)(2,1)} %get-tuple-element.8), channel_id=1, source_target_pairs={{0,3},{1,0},{2,1},{3,2},{4,7},{5,4},{6,5},{7,6},{8,11},{9,8},{10,9... | collective-permute-start | bytes 4718600 | tf_op jit(solution)/shard_map/ppermute | solution.py:265
  49.2 2.6 %all-to-all-done = bf16[64,8,128]{2,1,0:T(8,128)(2,1)S(1)} async-done(((bf16[64,8,128]{2,1,0:T(8,128)(2,1)}), bf16[64,8,128]{2,1,0:T(8,128)(2,1)S(1)}, u32[]{:S(2)}, u32[]{:S(2)}) %all-to-all-start) | async-done | bytes 131104 | tf_op jit(solution)/shard_map/all_to_all | solution.py:213
  51.7 0.0 copy-start
  51.7 0.0 copy-start.1
  51.7 1.1 spread.1
  52.9 6.8 %all-to-all-start.1 = ((bf16[16,256,128]{2,1,0:T(8,128)(2,1)}), bf16[16,256,128]{2,1,0:T(8,128)(2,1)S(1)}, u32[]{:S(2)}, u32[]{:S(2)}) async-start(bf16[16,256,128]{2,1,0:T(8,128)(2,1)} %spread.1), calls=%async_computation.1 | async-start | bytes 2097152 | tf_op jit(solution)/shard_map/all_to_all | solution.py:213
  59.7 8.3 %collective-permute-done.p0_hbm = bf16[3072,256]{1,0:T(8,128)(2,1)} collective-permute-done((bf16[3072,256]{1,0:T(8,128)(2,1)}, bf16[3072,256]{1,0:T(8,128)(2,1)}, u32[]{:S(2)}, u32[]{:S(2)}) %collective-permute-start) | collective-permute-done | bytes 1572896 | tf_op jit(solution)/shard_map/ppermute | solution.py:265
  68.0 8.0 %collective-permute-done.1.p1_hbm = bf16[3072,256]{1,0:T(8,128)(2,1)} collective-permute-done((bf16[3072,256]{1,0:T(8,128)(2,1)}, bf16[3072,256]{1,0:T(8,128)(2,1)}, u32[]{:S(2)}, u32[]{:S(2)}) %collective-permute-start.1) | collective-permute-done | bytes 1572896 | tf_op jit(solution)/shard_map/ppermute | solution.py:265
  76.0 1.4 all-to-all-done.1.tiles
  77.4 0.0 copy-done
  77.4 0.0 copy-done.1
  77.4 4.0 %ffn.1 = bf16[16,256,128]{2,1,0:T(8,128)(2,1)S(1)} custom-call(bf16[16,256,128]{2,1,0:T(8,128)(2,1)S(1)} %all-to-all-done.1.tiles, bf16[2048,256]{1,0:T(8,128)(2,1)S(1)} %bitcast.12, bf16[2048,256]{1,0:T(8,128)(2,1)S(1)} %bitcast.14, bf16[256,2048]{1,0:T(8,128)(2,1)} %bitcast.19, bf16[3072,256]{1,0:T(8,128)(2,1)} %collective-permute-done.p0_hbm, ...), custom_call_target="tpu_custom_call" | custom-call | flops 1610612736 | bytes 6291456 | tf_op jit(solution)/shard_map/ffn/pallas_call | solution.py:292
  81.4 0.0 copy-start.2
  81.4 21.5 %all_to_all.20.parts = bf16[16,256,128]{2,1,0:T(8,128)(2,1)S(1)} all-to-all(bf16[16,256,128]{2,1,0:T(8,128)(2,1)S(1)} %ffn.1), channel_id=1, replica_groups=mesh['ep'=64,'tp'=16] {'tp'}, dimensions={0} | all-to-all | bytes 2097152 | tf_op jit(solution)/shard_map/all_to_all | solution.py:213
  102.9 0.8 add.1
  103.6 26.0 %all-to-all-start.3 = ((bf16[64,8,128]{2,1,0:T(8,128)(2,1)}), bf16[64,8,128]{2,1,0:T(8,128)(2,1)S(1)}, u32[]{:S(2)}, u32[]{:S(2)}) async-start(bf16[64,8,128]{2,1,0:T(8,128)(2,1)} %bitcast.8), calls=%async_computation.3 | async-start | bytes 262144 | tf_op jit(solution)/shard_map/all_to_all | solution.py:213
  129.6 0.0 copy-done.2
  129.6 0.9 place.1.places
  130.6 11.4 %all-to-all-done.3 = bf16[64,8,128]{2,1,0:T(8,128)(2,1)S(1)} async-done(((bf16[64,8,128]{2,1,0:T(8,128)(2,1)}), bf16[64,8,128]{2,1,0:T(8,128)(2,1)S(1)}, u32[]{:S(2)}, u32[]{:S(2)}) %all-to-all-start.3) | async-done | bytes 131104 | tf_op jit(solution)/shard_map/all_to_all | solution.py:213
  142.0 0.9 combine.1
Async XLA Ops:
  1.9 49.9 %all-to-all-start = ((bf16[64,8,128]{2,1,0:T(8,128)(2,1)}), bf16[64,8,128]{2,1,0:T(8,128)(2,1)S(1)}, u32[]{:S(2)}, u32[]{:S(2)}) async-start(bf16[64,8,128]{2,1,0:T(8,128)(2,1)} %bitcast.3), calls=%async_computation | async-start | bytes 262144 | tf_op jit(solution)/shard_map/all_to_all | solution.py:213
  42.6 25.4 %collective-permute-start = (bf16[3072,256]{1,0:T(8,128)(2,1)}, bf16[3072,256]{1,0:T(8,128)(2,1)}, u32[]{:S(2)}, u32[]{:S(2)}) collective-permute-start(bf16[3072,256]{1,0:T(8,128)(2,1)} %get-tuple-element.7), channel_id=1, source_target_pairs={{0,1},{1,2},{2,3},{3,0},{4,5},{5,6},{6,7},{7,4},{8,9},{9,10},{10,1... | collective-permute-start | bytes 4718600 | tf_op jit(solution)/shard_map/ppermute | solution.py:265
  45.8 30.2 %collective-permute-start.1 = (bf16[3072,256]{1,0:T(8,128)(2,1)}, bf16[3072,256]{1,0:T(8,128)(2,1)}, u32[]{:S(2)}, u32[]{:S(2)}) collective-permute-start(bf16[3072,256]{1,0:T(8,128)(2,1)} %get-tuple-element.8), channel_id=1, source_target_pairs={{0,3},{1,0},{2,1},{3,2},{4,7},{5,4},{6,5},{7,6},{8,11},{9,8},{10,9... | collective-permute-start | bytes 4718600 | tf_op jit(solution)/shard_map/ppermute | solution.py:265
  51.7 25.7 %copy-start = (bf16[1,2048,256]{2,1,0:T(8,128)(2,1)S(1)}, bf16[1,2048,256]{2,1,0:T(8,128)(2,1)}, u32[]{:S(2)}) copy-start(bf16[1,2048,256]{2,1,0:T(8,128)(2,1)} %param.9) | copy-start | bytes 3145732
  51.7 25.7 %copy-start.1 = (bf16[1,2048,256]{2,1,0:T(8,128)(2,1)S(1)}, bf16[1,2048,256]{2,1,0:T(8,128)(2,1)}, u32[]{:S(2)}) copy-start(bf16[1,2048,256]{2,1,0:T(8,128)(2,1)} %param.10) | copy-start | bytes 3145732
  52.9 24.5 %all-to-all-start.1 = ((bf16[16,256,128]{2,1,0:T(8,128)(2,1)}), bf16[16,256,128]{2,1,0:T(8,128)(2,1)S(1)}, u32[]{:S(2)}, u32[]{:S(2)}) async-start(bf16[16,256,128]{2,1,0:T(8,128)(2,1)} %spread.1), calls=%async_computation.1 | async-start | bytes 2097152 | tf_op jit(solution)/shard_map/all_to_all | solution.py:213
  81.4 48.2 %copy-start.2 = (f32[1,64,8]{1,2,0:T(8,128)S(1)}, f32[1,64,8]{1,2,0:T(8,128)}, u32[]{:S(2)}) copy-start(f32[1,64,8]{1,2,0:T(8,128)} %param.8) | copy-start | bytes 6148
  103.6 38.3 %all-to-all-start.3 = ((bf16[64,8,128]{2,1,0:T(8,128)(2,1)}), bf16[64,8,128]{2,1,0:T(8,128)(2,1)S(1)}, u32[]{:S(2)}, u32[]{:S(2)}) async-start(bf16[64,8,128]{2,1,0:T(8,128)(2,1)} %bitcast.8), calls=%async_computation.3 | async-start | bytes 262144 | tf_op jit(solution)/shard_map/all_to_all | solution.py:213
